TPU v7x, 32 devices: a whole 2x2x4 slice. The times are simulated.
32 devices in a mesh: sp: 8 (over z, x), tp: 4 (over y, core).
Axes of the slice: x: 2, y: 2, z: 4, core: 2. Of those that a mesh axis runs over, the one named last changes fastest.
Arguments:
- tokens: bfloat16 [6144, 4096], P('sp', 'tp'), may hold values from -12 to 12
- query_weight: bfloat16 [4096, 2048], P(None, 'tp'), may hold values from -0.09375 to 0.09375
- key_weight: bfloat16 [4096, 2048], P(None, 'tp'), may hold values from -0.09375 to 0.09375
- value_weight: bfloat16 [4096, 2048], P(None, 'tp'), may hold values from -0.09375 to 0.09375
- position_bias: float32 [16, 320], P('tp'), may hold values from -104 to 154
- out_grad: bfloat16 [6144, 2048], P('sp', 'tp'), may hold values from -6 to 6
Outputs:
- input_grad: bfloat16 [6144, 4096], P('sp', 'tp')
- query_weight_grad: float32 [4096, 2048], P('sp', 'tp')
- key_weight_grad: float32 [4096, 2048], P('sp', 'tp')
- value_weight_grad: float32 [4096, 2048], P('sp', 'tp')
- bias_grad: float32 [16, 320], P('tp')
All inputs are finite; a program needn't handle non-finite values.
Results may differ from a plain program's by a relative error of at most 0.014.
Values may be sent and summed in bfloat16 or wider, within the bound.
A program may use at most 128 MiB of HBM per device.

v0:
```python
import functools

import jax
import jax.numpy as jnp
from jax import lax
from jax.experimental import pallas as pl
from jax.experimental.pallas import tpu as pltpu
from jax.sharding import PartitionSpec as P

SEGMENT = 64
PREVIOUS = 4
CLIP = 256
ROWS = 2 * SEGMENT
REACH = PREVIOUS * SEGMENT
WINDOW = ROWS + REACH
TABLE = 512
HIDDEN = -1e30


def from_behind(value, axis, steps):
    count = lax.axis_size(axis)
    leading, last = (max(0, -steps), min(count, count - steps))
    return lax.ppermute(value, axis, [(source, source + steps) for source in range(leading, last)])


def contract_rows(left, right):
    return lax.dot_general(
        left, right, (((0,), (0,)), ((), ())), preferred_element_type=jnp.float32
    )


def contract_cols(left, right):
    return lax.dot_general(
        left, right, (((1,), (1,)), ((), ())), preferred_element_type=jnp.float32
    )


def diagonal_sums(tile):
    half = tile.shape[0] // 2
    while half >= 8:
        tile = tile[:half] + pltpu.roll(tile[half:], TABLE - half, 1)
        half //= 2
    row = lax.broadcasted_iota(jnp.int32, tile.shape, 0)
    for step in (4, 2, 1):
        tile = jnp.where((row & step) != 0, pltpu.roll(tile, TABLE - step, 1), tile)
    return jnp.sum(tile, axis=0, keepdims=True)


def attention_kernel(
    factor,
    first_ref,
    q_ref,
    k_ref,
    v_ref,
    prev_ref,
    g_ref,
    table_ref,
    dq_ref,
    dk_ref,
    dv_ref,
    dk_tail_ref,
    dv_tail_ref,
    back_ref,
    table_grad_ref,
    k_all,
    v_all,
    dk_all,
    dv_all,
):
    length = q_ref.shape[0]
    k_all[:REACH] = prev_ref[0]
    k_all[REACH:] = k_ref[...]
    v_all[:REACH] = prev_ref[1]
    v_all[REACH:] = v_ref[...]
    dk_all[...] = jnp.zeros_like(dk_all)
    dv_all[...] = jnp.zeros_like(dv_all)
    first = first_ref[0]
    table = jnp.broadcast_to(table_ref[0], (ROWS, TABLE))
    bias = pltpu.roll(table, 0, 1, stride=1, stride_axis=0)[:, :WINDOW]
    row = lax.broadcasted_iota(jnp.int32, (ROWS, WINDOW), 0) // SEGMENT
    column = lax.broadcasted_iota(jnp.int32, (ROWS, WINDOW), 1)
    behind = column // SEGMENT - row
    bias = jnp.where((behind >= 0) & (behind <= PREVIOUS), bias, HIDDEN)
    bias_sum = jnp.zeros((ROWS, WINDOW), jnp.float32)
    for start in range(0, length, ROWS):
        q = q_ref[start : start + ROWS]
        g = g_ref[start : start + ROWS]
        k = k_all[start : start + WINDOW]
        v = v_all[start : start + WINDOW]
        mask = bias
        if start < REACH:
            mask = jnp.where(column + start < first, HIDDEN, bias)
        scores = contract_cols(q, k) * factor + mask
        top = jnp.max(scores, axis=1, keepdims=True)
        raised = jnp.exp(scores - top)
        weights = raised * (1.0 / jnp.sum(raised, axis=1, keepdims=True))
        prob_grad = contract_cols(g, v)
        delta = jnp.sum(weights * prob_grad, axis=1, keepdims=True)
        score_grad = weights * (prob_grad - delta)
        bias_sum = bias_sum + score_grad
        low = score_grad.astype(jnp.bfloat16)
        dq = jnp.dot(low, k, preferred_element_type=jnp.float32) * factor
        dq_ref[start : start + ROWS] = dq.astype(jnp.bfloat16)
        dk_all[start : start + WINDOW] += contract_rows(low, q)
        dv_all[start : start + WINDOW] += contract_rows(weights.astype(jnp.bfloat16), g)
    back_ref[0] = (dk_all[:REACH] * factor).astype(jnp.bfloat16)
    back_ref[1] = dv_all[:REACH].astype(jnp.bfloat16)
    dk_ref[...] = (dk_all[REACH:length] * factor).astype(jnp.bfloat16)
    dv_ref[...] = dv_all[REACH:length].astype(jnp.bfloat16)
    dk_tail_ref[...] = dk_all[length:] * factor
    dv_tail_ref[...] = dv_all[length:]
    padded = jnp.concatenate([bias_sum, jnp.zeros((ROWS, TABLE - WINDOW), jnp.float32)], axis=1)
    table_grad_ref[0] = diagonal_sums(padded)


def attention(query, keys, values, prev, out_grad, position_bias):
    length, width = query.shape
    heads, entries = position_bias.shape
    head = width // heads
    factor = head ** (-0.5)
    table = jnp.concatenate(
        [
            position_bias[:, ::-1],
            jnp.zeros((heads, WINDOW - entries), jnp.float32),
            jnp.broadcast_to(position_bias[:, entries - 1 :], (heads, TABLE - WINDOW)),
        ],
        axis=1,
    )[:, None]
    first = jnp.where(lax.axis_index("sp") == 0, REACH, 0).astype(jnp.int32)[None]

    def rows(count):
        return pl.BlockSpec((count, head), lambda h: (0, h))

    line = pl.BlockSpec((1, 1, TABLE), lambda h: (h, 0, 0))

    def shape(count, kind):
        return jax.ShapeDtypeStruct((count, width), kind)

    body = length - REACH
    elements = heads * length * WINDOW
    outs = pl.pallas_call(
        functools.partial(attention_kernel, factor),
        grid=(heads,),
        in_specs=[
            pl.BlockSpec(memory_space=pltpu.SMEM),
            rows(length),
            rows(length),
            rows(length),
            pl.BlockSpec((2, REACH, head), lambda h: (0, 0, h)),
            rows(length),
            line,
        ],
        out_specs=[
            rows(length),
            rows(body),
            rows(body),
            rows(REACH),
            rows(REACH),
            pl.BlockSpec((2, REACH, head), lambda h: (0, 0, h)),
            line,
        ],
        out_shape=[
            shape(length, jnp.bfloat16),
            shape(body, jnp.bfloat16),
            shape(body, jnp.bfloat16),
            shape(REACH, jnp.float32),
            shape(REACH, jnp.float32),
            jax.ShapeDtypeStruct((2, REACH, width), jnp.bfloat16),
            jax.ShapeDtypeStruct((heads, 1, TABLE), jnp.float32),
        ],
        scratch_shapes=[
            pltpu.VMEM((length + REACH, head), jnp.bfloat16),
            pltpu.VMEM((length + REACH, head), jnp.bfloat16),
            pltpu.VMEM((length + REACH, head), jnp.float32),
            pltpu.VMEM((length + REACH, head), jnp.float32),
        ],
        cost_estimate=pl.CostEstimate(
            flops=10 * elements * head, bytes_accessed=14 * length * width, transcendentals=elements
        ),
    )(first, query, keys, values, prev, out_grad, table)
    return outs


def table_to_bias(summed, entries):
    near = summed[:, 1:entries][:, ::-1]
    far = summed[:, :1] + jnp.sum(summed[:, WINDOW:], axis=1, keepdims=True)
    return jnp.concatenate([near, far], axis=1)


def ring_columns(count):
    columns = 1
    while (2 * columns) ** 2 <= count:
        columns *= 2
    return columns


def ring_place(index, count):
    columns = ring_columns(count)
    rows = count // columns
    row, column = index // columns, index % columns
    above = rows - 1 - row
    across = jnp.where(above % 2 == 0, column - 1, columns - 1 - column)
    return jnp.where(column == 0, row, rows + above * (columns - 1) + across)


def ring_index(place, count):
    columns = ring_columns(count)
    rows = count // columns
    later = jnp.maximum(place - rows, 0)
    above, across = later // (columns - 1), later % (columns - 1)
    column = jnp.where(above % 2 == 0, 1 + across, columns - 1 - across)
    return jnp.where(place < rows, place * columns, (rows - 1 - above) * columns + column)


def ring_kernel(
    count,
    whole_ref,
    dq_ref,
    dk_ref,
    dv_ref,
    line_ref,
    oq_ref,
    ok_ref,
    ov_ref,
    line_out_ref,
    sent,
    got,
    lines,
    send_sem,
    recv_sem,
    line_send,
    line_recv,
):
    me = lax.axis_index("sp")
    place = ring_place(me, count)
    barrier = pltpu.get_barrier_semaphore()
    for ahead in range(1, count):
        peer = lax.rem(me + ahead, count)
        pl.semaphore_signal(
            barrier, inc=1, device_id={"sp": peer}, device_id_type=pl.DeviceIdType.MESH
        )
    pl.semaphore_wait(barrier, count - 1)

    grads = (dq_ref, dk_ref, dv_ref)
    outs = (oq_ref, ok_ref, ov_ref)
    half = sent.shape[3]
    onward = (
        ring_index(lax.rem(place + 1, count), count),
        ring_index(lax.rem(place + count - 1, count), count),
    )

    def own(target, side, chain):
        start = pl.multiple_of((2 * ring_index(target, count) + side) * half, half)
        return contract_rows(whole_ref[:, pl.ds(start, half)], grads[chain][...])

    def target_of(step, side):
        if side == 0:
            return lax.rem(place - 1 - step + 2 * count, count)
        return lax.rem(place + 1 + step, count)

    def copy_of(step, side, chain):
        return pltpu.make_async_remote_copy(
            src_ref=sent.at[side, chain, step],
            dst_ref=got.at[side, chain, step],
            send_sem=send_sem.at[side, chain, step],
            recv_sem=recv_sem.at[side, chain, step],
            device_id={"sp": onward[side]},
            device_id_type=pl.DeviceIdType.MESH,
        )

    def line_copy(ahead):
        return pltpu.make_async_remote_copy(
            src_ref=line_ref,
            dst_ref=lines.at[ahead - 1],
            send_sem=line_send.at[ahead - 1],
            recv_sem=line_recv.at[ahead - 1],
            device_id={"sp": lax.rem(me + ahead, count)},
            device_id_type=pl.DeviceIdType.MESH,
        )

    chains = [(chain, side) for chain in range(3) for side in range(2)]
    for chain, side in chains:
        sent[side, chain, 0] = own(target_of(0, side), side, chain).astype(jnp.bfloat16)
        copy_of(0, side, chain).start()
    for ahead in range(1, count):
        line_copy(ahead).start()

    @pl.loop(1, count - 1)
    def _(step):
        for chain, side in chains:
            part = own(target_of(step, side), side, chain)
            copy_of(step - 1, side, chain).wait_recv()
            total = part + got[side, chain, step - 1].astype(jnp.float32)
            sent[side, chain, step] = total.astype(jnp.bfloat16)
            copy_of(step, side, chain).start()

    total = line_ref[...]
    for ahead in range(1, count):
        line_copy(ahead).wait()
        total = total + lines[ahead - 1]
    line_out_ref[...] = total
    for chain, side in chains:
        part = own(place, side, chain)
        copy_of(count - 2, side, chain).wait_recv()
        total = part + got[side, chain, count - 2].astype(jnp.float32)
        outs[chain][side * half : (side + 1) * half] = total

    @pl.loop(0, count - 1)
    def _(step):
        for chain, side in chains:
            copy_of(step, side, chain).wait_send()


def weight_grads(whole, query_grad, key_grad, value_grad, lines):
    count = lax.axis_size("sp")
    features = whole.shape[1]
    width = query_grad.shape[1]
    half = features // count // 2
    vmem = pl.BlockSpec(memory_space=pltpu.VMEM)
    out = jax.ShapeDtypeStruct((2 * half, width), jnp.float32)
    return pl.pallas_call(
        functools.partial(ring_kernel, count),
        in_specs=[vmem] * 5,
        out_specs=[vmem] * 4,
        out_shape=[out, out, out, jax.ShapeDtypeStruct(lines.shape, jnp.float32)],
        scratch_shapes=[
            pltpu.VMEM((2, 3, count - 1, half, width), jnp.bfloat16),
            pltpu.VMEM((2, 3, count - 1, half, width), jnp.bfloat16),
            pltpu.VMEM((count - 1,) + lines.shape, jnp.float32),
            pltpu.SemaphoreType.DMA((2, 3, count - 1)),
            pltpu.SemaphoreType.DMA((2, 3, count - 1)),
            pltpu.SemaphoreType.DMA((count - 1,)),
            pltpu.SemaphoreType.DMA((count - 1,)),
        ],
        compiler_params=pltpu.CompilerParams(
            collective_id=0, has_side_effects=True, vmem_limit_bytes=56 * 1024 * 1024
        ),
        cost_estimate=pl.CostEstimate(
            flops=6 * whole.shape[0] * features * width,
            bytes_accessed=400_000_000,
            transcendentals=0,
        ),
    )(whole, query_grad, key_grad, value_grad, lines)


def gather_kernel(
    parts,
    tokens_ref,
    wq_ref,
    wk_ref,
    wv_ref,
    whole_ref,
    q_ref,
    k_ref,
    v_ref,
    prev_ref,
    held,
    weights,
    total,
    halo,
    halo_got,
    side_send,
    side_recv,
    far_send,
    far_recv,
    relay_send,
    relay_recv,
    halo_send,
    halo_recv,
    load_sem,
    store_sem,
):
    me = lax.axis_index("tp")
    seat = lax.axis_index("sp")
    seats = lax.axis_size("sp")
    partner = me + 1 - 2 * lax.rem(me, 2)
    chunks = held.shape[0]
    block = tokens_ref.shape[1]
    width = q_ref.shape[1]
    pairs = parts // 2
    matrices = (wq_ref, wk_ref, wv_ref)

    def source(device, away):
        return lax.rem(device + parts - 2 * away, parts)

    order = [me, partner]
    for away in range(1, pairs):
        order += [source(me, away), source(partner, away)]

    def load(slot, matrix):
        start = pl.multiple_of(order[slot] * block, block)
        return pltpu.make_async_copy(
            matrices[matrix].at[pl.ds(start, block)],
            weights.at[slot, matrix],
            load_sem.at[slot, matrix],
        )

    for slot in range(parts):
        for matrix in range(3):
            load(slot, matrix).start()

    barrier = pltpu.get_barrier_semaphore()
    for ahead in range(1, parts):
        pl.semaphore_signal(
            barrier,
            inc=1,
            device_id={"tp": lax.rem(me + ahead, parts)},
            device_id_type=pl.DeviceIdType.MESH,
        )
    onward = lax.rem(seat + 1, seats)
    for other in (onward, lax.rem(seat + seats - 1, seats)):
        pl.semaphore_signal(
            barrier, inc=1, device_id={"sp": other}, device_id_type=pl.DeviceIdType.MESH
        )
    pl.semaphore_wait(barrier, parts + 1)

    def rows(chunk):
        return pl.ds(chunk * REACH, REACH)

    def remote(src, dst, send, recv, device):
        return pltpu.make_async_remote_copy(
            src_ref=src,
            dst_ref=dst,
            send_sem=send,
            recv_sem=recv,
            device_id=device,
            device_id_type=pl.DeviceIdType.MESH,
        )

    def far(chunk, away):
        return remote(
            tokens_ref.at[rows(chunk)],
            held.at[chunk, me],
            far_send.at[chunk, away - 1],
            far_recv.at[chunk, away - 1],
            {"tp": lax.rem(me + 2 * away, parts)},
        )

    def side(chunk):
        return remote(
            tokens_ref.at[rows(chunk)],
            held.at[chunk, me],
            side_send.at[chunk],
            side_recv.at[chunk],
            {"tp": partner},
        )

    def relay(chunk, away):
        place = held.at[chunk, source(me, away)]
        return remote(
            place,
            place,
            relay_send.at[chunk, away - 1],
            relay_recv.at[chunk, away - 1],
            {"tp": partner},
        )

    def neighbour():
        return remote(halo, halo_got, halo_send, halo_recv, {"sp": onward})

    def store(chunk, slot):
        start = pl.multiple_of(order[slot] * block, block)
        src = tokens_ref.at[rows(chunk)] if slot == 0 else held.at[chunk, order[slot]]
        return pltpu.make_async_copy(
            src, whole_ref.at[rows(chunk), pl.ds(start, block)], store_sem.at[chunk, slot]
        )

    def add(chunk, slot, value):
        for matrix in range(3):
            term = jnp.dot(value, weights[slot, matrix], preferred_element_type=jnp.float32)
            if slot == 0:
                total[matrix, chunk] = term
            else:
                total[matrix, chunk] += term

    backwards = list(range(chunks))[::-1]
    for chunk in backwards:
        for away in range(1, pairs):
            far(chunk, away).start()
        side(chunk).start()
    for slot in range(2):
        for matrix in range(3):
            load(slot, matrix).wait()
        for chunk in backwards:
            if slot == 1:
                side(chunk).wait_recv()
            store(chunk, slot).start()
            value = tokens_ref[rows(chunk)] if slot == 0 else held[chunk, partner]
            add(chunk, slot, value)
    for slot in range(2, parts):
        for matrix in range(3):
            load(slot, matrix).wait()
    outs = (q_ref, k_ref, v_ref)
    for chunk in backwards:
        for away in range(1, pairs):
            far(chunk, away).wait_recv()
            relay(chunk, away).start()
            store(chunk, 2 * away).start()
            add(chunk, 2 * away, held[chunk, source(me, away)])
        for away in range(1, pairs):
            relay(chunk, away).wait_recv()
            store(chunk, 2 * away + 1).start()
            add(chunk, 2 * away + 1, held[chunk, source(partner, away)])
        for matrix in range(3):
            outs[matrix][rows(chunk)] = total[matrix, chunk].astype(jnp.bfloat16)
        if chunk == chunks - 1:
            halo[0] = total[1, chunk].astype(jnp.bfloat16)
            halo[1] = total[2, chunk].astype(jnp.bfloat16)
            neighbour().start()
    neighbour().wait()
    prev_ref[...] = halo_got[...]
    for chunk in backwards:
        side(chunk).wait_send()
        for away in range(1, pairs):
            far(chunk, away).wait_send()
            relay(chunk, away).wait_send()
        for slot in range(parts):
            store(chunk, slot).wait()


def project(tokens, query_weight, key_weight, value_weight):
    parts = lax.axis_size("tp")
    length, block = tokens.shape
    width = query_weight.shape[1]
    chunks = length // REACH
    pairs = parts // 2
    vmem = pl.BlockSpec(memory_space=pltpu.VMEM)
    anywhere = pl.BlockSpec(memory_space=pl.ANY)
    narrow = jax.ShapeDtypeStruct((length, width), jnp.bfloat16)
    dma = pltpu.SemaphoreType.DMA
    return pl.pallas_call(
        functools.partial(gather_kernel, parts),
        in_specs=[vmem, anywhere, anywhere, anywhere],
        out_specs=[anywhere, vmem, vmem, vmem, vmem],
        out_shape=[
            jax.ShapeDtypeStruct((length, block * parts), jnp.bfloat16),
            narrow,
            narrow,
            narrow,
            jax.ShapeDtypeStruct((2, REACH, width), jnp.bfloat16),
        ],
        scratch_shapes=[
            pltpu.VMEM((chunks, parts, REACH, block), jnp.bfloat16),
            pltpu.VMEM((parts, 3, block, width), jnp.bfloat16),
            pltpu.VMEM((3, chunks, REACH, width), jnp.float32),
            pltpu.VMEM((2, REACH, width), jnp.bfloat16),
            pltpu.VMEM((2, REACH, width), jnp.bfloat16),
            dma((chunks,)),
            dma((chunks,)),
            dma((chunks, pairs - 1)),
            dma((chunks, pairs - 1)),
            dma((chunks, pairs - 1)),
            dma((chunks, pairs - 1)),
            dma(()),
            dma(()),
            dma((parts, 3)),
            dma((chunks, parts)),
        ],
        compiler_params=pltpu.CompilerParams(
            collective_id=1, has_side_effects=True, vmem_limit_bytes=56 * 1024 * 1024
        ),
        cost_estimate=pl.CostEstimate(
            flops=6 * length * block * parts * width, bytes_accessed=150_000_000, transcendentals=0
        ),
    )(tokens, query_weight, key_weight, value_weight)


def shards(tokens, query_weight, key_weight, value_weight, position_bias, out_grad):
    weights = jnp.concatenate([query_weight, key_weight, value_weight], axis=1)
    whole, query, keys, values, prev = project(tokens, query_weight, key_weight, value_weight)
    query_grad, key_body, value_body, key_tail, value_tail, back, lines = attention(
        query, keys, values, prev, out_grad, position_bias
    )
    after = from_behind(back, "sp", -1)
    key_grad = jnp.concatenate([key_body, (key_tail + after[0]).astype(jnp.bfloat16)])
    value_grad = jnp.concatenate([value_body, (value_tail + after[1]).astype(jnp.bfloat16)])
    grads = jnp.concatenate([query_grad, key_grad, value_grad], axis=1)
    input_part = contract_cols(grads, weights).astype(jnp.bfloat16)
    input_grad = lax.psum_scatter(input_part, "tp", scatter_dimension=1, tiled=True)
    barrier = lax.optimization_barrier((key_grad, input_part))
    query_weight_grad, key_weight_grad, value_weight_grad, lines = weight_grads(
        whole, query_grad, barrier[0], value_grad, lines[:, 0]
    )
    bias_grad = table_to_bias(lines, position_bias.shape[1])
    return input_grad, query_weight_grad, key_weight_grad, value_weight_grad, bias_grad


def solution(mesh):
    in_specs = (
        P("sp", "tp"),
        P(None, "tp"),
        P(None, "tp"),
        P(None, "tp"),
        P("tp", None),
        P("sp", "tp"),
    )
    out_specs = (P("sp", "tp"), P("sp", "tp"), P("sp", "tp"), P("sp", "tp"), P("tp", None))
    return jax.shard_map(shards, mesh=mesh, in_specs=in_specs, out_specs=out_specs, check_vma=False)
```

profile of v0, /device:TPU:0, one launch (start us, length us, event | category | flops | bytes accessed | tf_op | source)
XLA Modules:
  0.0 256.7 jit_solution(14970227267842754484)
XLA Ops:
  7.2 0.0 reduce-scatter.2.cloned.1.call-start
  7.2 0.9 slice_reduce_fusion.1
  8.1 1.5 reverse
  9.6 0.1 slice.35
  9.7 0.1 pad.15.clone
  9.8 0.1 broadcast_in_dim.22
  9.9 0.6 broadcast_in_dim.23.table_ref
  10.5 47.0 %shard_map.101 = (bf16[768,4096]{1,0:T(8,128)(2,1)}, bf16[768,512]{1,0:T(8,128)(2,1)}, bf16[768,512]{1,0:T(8,128)(2,1)}, bf16[768,512]{1,0:T(8,128)(2,1)}, bf16[2,256,512]{2,1,0:T(8,128)(2,1)}) custom-call(bf16[768,1024]{1,0:T(8,128)(2,1)} %tokens_ref.1, bf16[4096,512]{1,0:T(8,128)(2,1)} %wq_ref.1, bf16[4096,512]{1,0:T(8,128)(2,1)} %wk_ref.1, ...), custom_call_target="tpu_custom_call" | custom-call | flops 9663676416 | bytes 150000000 | tf_op jit(solution)/shard_map/pallas_call | solution.py:531
  57.4 17.1 %shard_map.102 = (bf16[768,512]{1,0:T(8,128)(2,1)}, bf16[512,512]{1,0:T(8,128)(2,1)}, bf16[512,512]{1,0:T(8,128)(2,1)}, f32[256,512]{1,0:T(8,128)}, f32[256,512]...) custom-call(s32[1]{0:T(128)} %bitcast.first_ref, bf16[768,512]{1,0:T(8,128)(2,1)} %get-tuple-element.22.q_ref, ...), custom_call_target="tpu_custom_call" | custom-call | flops 1509949440 | bytes 5505024 | tf_op jit(solution)/shard_map/pallas_call | solution.py:141
  74.6 1.5 collective-permute-start
  76.1 15.3 %collective-permute-done = bf16[2,256,512]{2,1,0:T(8,128)(2,1)S(1)} collective-permute-done((bf16[2,256,512]{2,1,0:T(8,128)(2,1)}, bf16[2,256,512]{2,1,0:T(8,128)(2,1)S(1)}, u32[]{:S(2)}, u32[]{:S(2)}) %collective-permute-start) | collective-permute-done | bytes 524320 | tf_op jit(solution)/shard_map/ppermute | solution.py:23
  91.4 1.4 fusion.19
  92.8 15.2 %fusion.6 = bf16[768,4096]{1,0:T(8,128)(2,1)} fusion(bf16[4096,512]{1,0:T(8,128)(2,1)} %wv_ref.1, bf16[4096,512]{1,0:T(8,128)(2,1)} %wk_ref.1, bf16[4096,512]{1,0:T(8,128)(2,1)} %wq_ref.1, bf16[256,512]{1,0:T(8,128)(2,1)S(1)} %get-tuple-element.40, bf16[512,512]{1,0:T(8,128)(2,1)} %get-tuple-element.30, bf16[256,512]{1,0:T(8,128)(2,1)S(1)} %get-tuple-element.39, ...), kind=kOutput, calls=%fused_computation.6 | convolution fusion | flops 9716367360 | bytes 21233664 | tf_op jit(solution)/shard_map/dot_general | solution.py:33
  108.0 0.0 reduce-scatter.2.cloned.1.call-update
  108.0 0.7 copy-done.3
  108.7 0.6 copy.14
  109.3 0.0 copy-done.1
  109.3 0.0 copy-done.2
  109.3 1.2 pad_maximum_fusion
  110.5 130.4 %shard_map.103 = (f32[512,512]{1,0:T(8,128)}, f32[512,512]{1,0:T(8,128)}, f32[512,512]{1,0:T(8,128)}, f32[4,512]{1,0:T(4,128)}) custom-call(bf16[768,4096]{1,0:T(8,128)(2,1)} %get-tuple-element.32.whole_ref, bf16[768,512]{1,0:T(8,128)(2,1)} %get-tuple-element.26.dq_ref, bf16[768,512]{1,0:T(8,128)(2,1)} %get-tuple-element.33.dk_ref, ...), custom_call_target="tpu_custom_call" | custom-call | flops 9663676416 | bytes 400000000 | tf_op jit(solution)/shard_map/pallas_call | solution.py:321
  240.9 0.0 copy-start
  241.0 0.9 slice.21
  241.8 0.7 slice_reduce_fusion
  242.6 0.1 copy.11
  242.7 0.3 reverse.1
  242.9 0.1 slice.36
  243.0 0.7 slice_add_fusion
  243.7 0.7 pad_maximum_fusion.3
  244.3 2.3 copy.18
  246.6 2.3 copy.19
  248.9 0.0 copy-done
  248.9 1.0 copy.20
  (6 shorter events, 0.0 us)
Async XLA Ops:
  7.2 237.2 %reduce-scatter.2.cloned.1.call-start = ((), (), s32[]{:S(2)}) async-start(), calls=%async_computation.1 | async-start | bytes 7864320 | tf_op jit(solution)/shard_map/reduce_scatter | solution.py:579
  74.6 16.8 %collective-permute-start = (bf16[2,256,512]{2,1,0:T(8,128)(2,1)}, bf16[2,256,512]{2,1,0:T(8,128)(2,1)S(1)}, u32[]{:S(2)}, u32[]{:S(2)}) collective-permute-start(bf16[2,256,512]{2,1,0:T(8,128)(2,1)} %get-tuple-element.29), channel_id=1, source_target_pairs={{4,0},{8,4},{12,8},{16,12},{20,16},{24,20},{28,24},{5,1},{9,5},{13... | collective-permute-start | bytes 1572872 | tf_op jit(solution)/shard_map/ppermute | solution.py:23
  108.0 0.7 copy-start.3
  108.0 1.3 copy-start.1
  108.0 1.3 copy-start.2
  240.9 7.9 %copy-start = (f32[512,512]{1,0:T(8,128)S(1)}, f32[512,512]{1,0:T(8,128)}, u32[]{:S(2)}) copy-start(f32[512,512]{1,0:T(8,128)} %get-tuple-element.51) | copy-start | bytes 3145732
Sparse Core Ops, SparseCore 0:
  108.1 55.6 reduce-scatter.1
where the time goes:
time: 257 us
  Pallas kernels  195 us (76%)
  waiting for transfers between devices  15.4 us (6%)
  matrix products  15.2 us (6%)
  between operations  14.1 us (5%)
  local copies, waits for them, and re-layouts  11.3 us (4%)
  other arithmetic  4.7 us (2%)
    pallas_call x1, Pallas kernels, weight_grads(): pl.pallas_call(functools.partial(ring_kernel, count), in_specs=[vmem] * 5...  130 us
    pallas_call x1, Pallas kernels, project(): pl.pallas_call(functools.partial(gather_kernel, parts), in_specs=[vmem, a...  47 us
    pallas_call x1, Pallas kernels, attention(): pl.pallas_call(functools.partial(attention_kernel, factor), grid=(heads,)...  17.1 us
    ppermute x1, waiting for transfers between devices, from_behind(): lax.ppermute(value, axis, [(source, source + steps) for source in range(l...  15.3 us
    dot_general x1, matrix products, contract_cols(): lax.dot_general(left, right, (((1,), (1,)), ((), ())), preferred_element_...  15.2 us
    unnamed x16, local copies, waits for them, and re-layouts  8.72 us
  transfers between devices with their start and end apart: 2, of which 1 were waited for; matrix products, arithmetic and copies ran while one was open for 2% of the time, Pallas kernels for 51%

commit v1 on v0

--- a/solution.py
+++ b/solution.py
@@ -15,12 +15,6 @@
 WINDOW = ROWS + REACH
 TABLE = 512
 HIDDEN = -1e30
-
-
-def from_behind(value, axis, steps):
-    count = lax.axis_size(axis)
-    leading, last = (max(0, -steps), min(count, count - steps))
-    return lax.ppermute(value, axis, [(source, source + steps) for source in range(leading, last)])
 
 
 def contract_rows(left, right):
@@ -214,133 +208,361 @@
 
 def ring_kernel(
     count,
-    whole_ref,
-    dq_ref,
-    dk_ref,
-    dv_ref,
+    parts,
+    whole_hbm,
+    dq_hbm,
+    dk_hbm,
+    dv_hbm,
+    dk_tail_ref,
+    dv_tail_ref,
+    back_ref,
     line_ref,
+    wq_hbm,
+    wk_hbm,
+    wv_hbm,
+    input_ref,
     oq_ref,
     ok_ref,
     ov_ref,
     line_out_ref,
+    whole,
+    grads,
+    weights,
+    after,
     sent,
     got,
     lines,
+    pair_sent,
+    pair_got,
+    cross_sent,
+    cross_got,
+    kept,
+    load_sem,
+    back_send,
+    back_recv,
     send_sem,
     recv_sem,
     line_send,
     line_recv,
+    pair_send,
+    pair_recv,
+    cross_send,
+    cross_recv,
 ):
     me = lax.axis_index("sp")
+    seat = lax.axis_index("tp")
+    core = lax.rem(seat, 2)
+    row = seat // 2
+    pairs = parts // 2
+    partner = seat + 1 - 2 * core
     place = ring_place(me, count)
+    length = whole.shape[0]
+    body = length - REACH
+    block = input_ref.shape[1]
+    bands = length // REACH
+
+    loads = [
+        pltpu.make_async_copy(whole_hbm, whole, load_sem.at[0]),
+        pltpu.make_async_copy(dq_hbm, grads.at[0], load_sem.at[1]),
+        pltpu.make_async_copy(dk_hbm, grads.at[1, pl.ds(0, body)], load_sem.at[2]),
+        pltpu.make_async_copy(dv_hbm, grads.at[2, pl.ds(0, body)], load_sem.at[3]),
+        pltpu.make_async_copy(wq_hbm, weights.at[0], load_sem.at[4]),
+        pltpu.make_async_copy(wk_hbm, weights.at[1], load_sem.at[5]),
+        pltpu.make_async_copy(wv_hbm, weights.at[2], load_sem.at[6]),
+    ]
+    for load in loads:
+        load.start()
+
     barrier = pltpu.get_barrier_semaphore()
     for ahead in range(1, count):
         peer = lax.rem(me + ahead, count)
         pl.semaphore_signal(
             barrier, inc=1, device_id={"sp": peer}, device_id_type=pl.DeviceIdType.MESH
         )
-    pl.semaphore_wait(barrier, count - 1)
-
-    grads = (dq_ref, dk_ref, dv_ref)
+    for ahead in range(1, parts):
+        peer = lax.rem(seat + ahead, parts)
+        pl.semaphore_signal(
+            barrier, inc=1, device_id={"tp": peer}, device_id_type=pl.DeviceIdType.MESH
+        )
+    pl.semaphore_wait(barrier, count + parts - 2)
+
     outs = (oq_ref, ok_ref, ov_ref)
-    half = sent.shape[3]
+    half = got.shape[3]
     onward = (
         ring_index(lax.rem(place + 1, count), count),
         ring_index(lax.rem(place + count - 1, count), count),
     )
 
+    def remote(src, dst, send, recv, device):
+        return pltpu.make_async_remote_copy(
+            src_ref=src,
+            dst_ref=dst,
+            send_sem=send,
+            recv_sem=recv,
+            device_id=device,
+            device_id_type=pl.DeviceIdType.MESH,
+        )
+
     def own(target, side, chain):
         start = pl.multiple_of((2 * ring_index(target, count) + side) * half, half)
-        return contract_rows(whole_ref[:, pl.ds(start, half)], grads[chain][...])
+        return contract_rows(whole[:, pl.ds(start, half)], grads[chain])
 
     def target_of(step, side):
         if side == 0:
             return lax.rem(place - 1 - step + 2 * count, count)
         return lax.rem(place + 1 + step, count)
 
+    def first_copy(side, chain):
+        return remote(
+            sent.at[side, chain],
+            got.at[side, chain, 0],
+            send_sem.at[side, chain, 0],
+            recv_sem.at[side, chain, 0],
+            {"sp": onward[side]},
+        )
+
     def copy_of(step, side, chain):
-        return pltpu.make_async_remote_copy(
-            src_ref=sent.at[side, chain, step],
-            dst_ref=got.at[side, chain, step],
-            send_sem=send_sem.at[side, chain, step],
-            recv_sem=recv_sem.at[side, chain, step],
-            device_id={"sp": onward[side]},
-            device_id_type=pl.DeviceIdType.MESH,
+        return remote(
+            got.at[side, chain, step - 1],
+            got.at[side, chain, step],
+            send_sem.at[side, chain, step],
+            recv_sem.at[side, chain, step],
+            {"sp": onward[side]},
+        )
+
+    def received(step, side, chain):
+        return remote(
+            sent.at[side, chain],
+            got.at[side, chain, step],
+            send_sem.at[side, chain, step],
+            recv_sem.at[side, chain, step],
+            {"sp": onward[side]},
         )
 
     def line_copy(ahead):
-        return pltpu.make_async_remote_copy(
-            src_ref=line_ref,
-            dst_ref=lines.at[ahead - 1],
-            send_sem=line_send.at[ahead - 1],
-            recv_sem=line_recv.at[ahead - 1],
-            device_id={"sp": lax.rem(me + ahead, count)},
-            device_id_type=pl.DeviceIdType.MESH,
-        )
-
-    chains = [(chain, side) for chain in range(3) for side in range(2)]
-    for chain, side in chains:
-        sent[side, chain, 0] = own(target_of(0, side), side, chain).astype(jnp.bfloat16)
-        copy_of(0, side, chain).start()
+        return remote(
+            line_ref,
+            lines.at[ahead - 1],
+            line_send.at[ahead - 1],
+            line_recv.at[ahead - 1],
+            {"sp": lax.rem(me + ahead, count)},
+        )
+
+    def back_copy(which):
+        return remote(
+            back_ref.at[which],
+            after.at[which],
+            back_send.at[which],
+            back_recv.at[which],
+            {"sp": lax.rem(me + count - 1, count)},
+        )
+
+    def rows(band):
+        return pl.ds(pl.multiple_of(band * REACH, REACH), REACH)
+
+    def part(band, target):
+        start = pl.multiple_of(target * block, block)
+        term = contract_cols(grads[0, rows(band)], weights[0, pl.ds(start, block)])
+        term += contract_cols(grads[1, rows(band)], weights[1, pl.ds(start, block)])
+        return term + contract_cols(grads[2, rows(band)], weights[2, pl.ds(start, block)])
+
+    def pair_copy(band, away):
+        return remote(
+            pair_sent.at[band, away],
+            pair_got.at[band, away],
+            pair_send.at[band, away],
+            pair_recv.at[band, away],
+            {"tp": partner},
+        )
+
+    def cross_copy(band, away):
+        return remote(
+            cross_sent.at[band, away - 1],
+            cross_got.at[band, away - 1],
+            cross_send.at[band, away - 1],
+            cross_recv.at[band, away - 1],
+            {"tp": lax.rem(seat + 2 * away, parts)},
+        )
+
+    def to_partner(band):
+        for away in range(pairs):
+            target = 2 * lax.rem(row + away, pairs) + 1 - core
+            pair_sent[band, away] = part(band, target).astype(jnp.bfloat16)
+            pair_copy(band, away).start()
+
+    def across(band):
+        for away in range(1, pairs):
+            term = part(band, lax.rem(seat + 2 * away, parts))
+            pair_copy(band, away).wait_recv()
+            term = term + pair_got[band, away].astype(jnp.float32)
+            cross_sent[band, away - 1] = term.astype(jnp.bfloat16)
+            cross_copy(band, away).start()
+        term = part(band, seat)
+        pair_copy(band, 0).wait_recv()
+        kept[band] = term + pair_got[band, 0].astype(jnp.float32)
+
+    def finish(band):
+        term = kept[band]
+        for away in range(1, pairs):
+            cross_copy(band, away).wait_recv()
+            term = term + cross_got[band, away - 1].astype(jnp.float32)
+        input_ref[rows(band)] = term.astype(jnp.bfloat16)
+
+    def work(unit):
+        band = unit // 2
+
+        @pl.when(lax.rem(unit, 2) == 0)
+        def _():
+            to_partner(band)
+
+        @pl.when(lax.rem(unit, 2) == 1)
+        def _():
+            across(band)
+
+        @pl.when((lax.rem(unit, 2) == 1) & (unit > 2))
+        def _():
+            finish(band - 1)
+
+    @pl.when(me > 0)
+    def _():
+        back_copy(0).start()
+        back_copy(1).start()
+
+    loads[0].wait()
+    loads[1].wait()
+    tails = (dk_tail_ref, dv_tail_ref)
+    for chain in range(3):
+        if chain > 0:
+            which = chain - 1
+
+            @pl.when(me < count - 1)
+            def _():
+                back_copy(which).wait_recv()
+
+            @pl.when(me == count - 1)
+            def _():
+                after[which] = jnp.zeros_like(after[which])
+
+            loads[1 + chain].wait()
+            tail = tails[which][...] + after[which].astype(jnp.float32)
+            grads[chain, body:] = tail.astype(jnp.bfloat16)
+        for side in range(2):
+            sent[side, chain] = own(target_of(0, side), side, chain).astype(jnp.bfloat16)
+            first_copy(side, chain).start()
     for ahead in range(1, count):
         line_copy(ahead).start()
+    for matrix in range(3):
+        loads[4 + matrix].wait()
+
+    units = 2 * bands
+    chains = [(chain, side) for chain in range(3) for side in range(2)]
 
     @pl.loop(1, count - 1)
     def _(step):
         for chain, side in chains:
-            part = own(target_of(step, side), side, chain)
-            copy_of(step - 1, side, chain).wait_recv()
-            total = part + got[side, chain, step - 1].astype(jnp.float32)
-            sent[side, chain, step] = total.astype(jnp.bfloat16)
+            part_of = own(target_of(step, side), side, chain)
+            received(step - 1, side, chain).wait_recv()
+            total = part_of + got[side, chain, step - 1].astype(jnp.float32)
+            got[side, chain, step - 1] = total.astype(jnp.bfloat16)
             copy_of(step, side, chain).start()
-
+            if (chain, side) == (1, 1):
+
+                @pl.when(step <= units)
+                def _():
+                    work(step - 1)
+
+    for unit in range(min(count - 2, units), units):
+        work(unit)
     total = line_ref[...]
     for ahead in range(1, count):
         line_copy(ahead).wait()
         total = total + lines[ahead - 1]
     line_out_ref[...] = total
     for chain, side in chains:
-        part = own(place, side, chain)
-        copy_of(count - 2, side, chain).wait_recv()
-        total = part + got[side, chain, count - 2].astype(jnp.float32)
+        if (chain, side) == (2, 0):
+            finish(bands - 1)
+        part_of = own(place, side, chain)
+        received(count - 2, side, chain).wait_recv()
+        total = part_of + got[side, chain, count - 2].astype(jnp.float32)
         outs[chain][side * half : (side + 1) * half] = total
+
+    @pl.when(me > 0)
+    def _():
+        back_copy(0).wait_send()
+        back_copy(1).wait_send()
 
     @pl.loop(0, count - 1)
     def _(step):
         for chain, side in chains:
-            copy_of(step, side, chain).wait_send()
-
-
-def weight_grads(whole, query_grad, key_grad, value_grad, lines):
+            received(step, side, chain).wait_send()
+
+    @pl.loop(0, bands)
+    def _(band):
+        for away in range(pairs):
+            pair_copy(band, away).wait_send()
+        for away in range(1, pairs):
+            cross_copy(band, away).wait_send()
+
+
+def final_grads(whole, grads, tails, back, lines, weights):
     count = lax.axis_size("sp")
-    features = whole.shape[1]
-    width = query_grad.shape[1]
+    parts = lax.axis_size("tp")
+    pairs = parts // 2
+    length, features = whole.shape
+    width = weights[0].shape[1]
     half = features // count // 2
+    block = features // parts
+    bands = length // REACH
     vmem = pl.BlockSpec(memory_space=pltpu.VMEM)
+    anywhere = pl.BlockSpec(memory_space=pl.ANY)
     out = jax.ShapeDtypeStruct((2 * half, width), jnp.float32)
+    dma = pltpu.SemaphoreType.DMA
+    low = jnp.bfloat16
     return pl.pallas_call(
-        functools.partial(ring_kernel, count),
-        in_specs=[vmem] * 5,
-        out_specs=[vmem] * 4,
-        out_shape=[out, out, out, jax.ShapeDtypeStruct(lines.shape, jnp.float32)],
+        functools.partial(ring_kernel, count, parts),
+        in_specs=[anywhere] * 4 + [vmem] * 4 + [anywhere] * 3,
+        out_specs=[vmem] * 5,
+        out_shape=[
+            jax.ShapeDtypeStruct((length, block), low),
+            out,
+            out,
+            out,
+            jax.ShapeDtypeStruct(lines.shape, jnp.float32),
+        ],
         scratch_shapes=[
-            pltpu.VMEM((2, 3, count - 1, half, width), jnp.bfloat16),
-            pltpu.VMEM((2, 3, count - 1, half, width), jnp.bfloat16),
+            pltpu.VMEM((length, features), low),
+            pltpu.VMEM((3, length, width), low),
+            pltpu.VMEM((3, features, width), low),
+            pltpu.VMEM((2, REACH, width), low),
+            pltpu.VMEM((2, 3, half, width), low),
+            pltpu.VMEM((2, 3, count - 1, half, width), low),
             pltpu.VMEM((count - 1,) + lines.shape, jnp.float32),
-            pltpu.SemaphoreType.DMA((2, 3, count - 1)),
-            pltpu.SemaphoreType.DMA((2, 3, count - 1)),
-            pltpu.SemaphoreType.DMA((count - 1,)),
-            pltpu.SemaphoreType.DMA((count - 1,)),
+            pltpu.VMEM((bands, pairs, REACH, block), low),
+            pltpu.VMEM((bands, pairs, REACH, block), low),
+            pltpu.VMEM((bands, pairs - 1, REACH, block), low),
+            pltpu.VMEM((bands, pairs - 1, REACH, block), low),
+            pltpu.VMEM((bands, REACH, block), jnp.float32),
+            dma((7,)),
+            dma((2,)),
+            dma((2,)),
+            dma((2, 3, count - 1)),
+            dma((2, 3, count - 1)),
+            dma((count - 1,)),
+            dma((count - 1,)),
+            dma((bands, pairs)),
+            dma((bands, pairs)),
+            dma((bands, pairs - 1)),
+            dma((bands, pairs - 1)),
         ],
         compiler_params=pltpu.CompilerParams(
-            collective_id=0, has_side_effects=True, vmem_limit_bytes=56 * 1024 * 1024
+            collective_id=0, has_side_effects=True, vmem_limit_bytes=63 * 1024 * 1024
         ),
         cost_estimate=pl.CostEstimate(
-            flops=6 * whole.shape[0] * features * width,
+            flops=12 * length * features * width,
             bytes_accessed=400_000_000,
             transcendentals=0,
         ),
-    )(whole, query_grad, key_grad, value_grad, lines)
+    )(whole, *grads, *tails, back, lines, *weights)
 
 
 def gather_kernel(
@@ -566,20 +788,17 @@
 
 
 def shards(tokens, query_weight, key_weight, value_weight, position_bias, out_grad):
-    weights = jnp.concatenate([query_weight, key_weight, value_weight], axis=1)
     whole, query, keys, values, prev = project(tokens, query_weight, key_weight, value_weight)
     query_grad, key_body, value_body, key_tail, value_tail, back, lines = attention(
         query, keys, values, prev, out_grad, position_bias
     )
-    after = from_behind(back, "sp", -1)
-    key_grad = jnp.concatenate([key_body, (key_tail + after[0]).astype(jnp.bfloat16)])
-    value_grad = jnp.concatenate([value_body, (value_tail + after[1]).astype(jnp.bfloat16)])
-    grads = jnp.concatenate([query_grad, key_grad, value_grad], axis=1)
-    input_part = contract_cols(grads, weights).astype(jnp.bfloat16)
-    input_grad = lax.psum_scatter(input_part, "tp", scatter_dimension=1, tiled=True)
-    barrier = lax.optimization_barrier((key_grad, input_part))
-    query_weight_grad, key_weight_grad, value_weight_grad, lines = weight_grads(
-        whole, query_grad, barrier[0], value_grad, lines[:, 0]
+    input_grad, query_weight_grad, key_weight_grad, value_weight_grad, lines = final_grads(
+        whole,
+        (query_grad, key_body, value_body),
+        (key_tail, value_tail),
+        back,
+        lines[:, 0],
+        (query_weight, key_weight, value_weight),
     )
     bias_grad = table_to_bias(lines, position_bias.shape[1])
     return input_grad, query_weight_grad, key_weight_grad, value_weight_grad, bias_grad

time: 257 us -> 219 us (0.85)
  waiting for transfers between devices: 15.4 us -> 0 us
  matrix products: 15.2 us -> 0 us
  between operations: 14.1 us -> 0.69 us
  Pallas kernels: 195 us -> 203 us
    ppermute x1 -> x0, waiting for transfers between devices: 15.3 us -> none  [from_behind(): lax.ppermute(value, axis, [(source, source + steps) for source in range(l...]
    dot_general x1 -> x0, matrix products: 15.2 us -> none  [contract_cols(): lax.dot_general(left, right, (((1,), (1,)), ((), ())), preferred_element_...]
    pallas_call x1, Pallas kernels: 130 us -> 139 us  [final_grads(): pl.pallas_call(functools.partial(ring_kernel, count, parts), in_specs=[an...]
    unnamed x16 -> x13, local copies, waits for them, and re-layouts: 8.72 us -> 10.1 us
  transfers between devices with their start and end apart: 2 -> 0, of which waited for: 1 -> 0; matrix products, arithmetic and copies ran while one was open for 2% -> 0% of each run, Pallas kernels for 51% -> 0%
where the time goes in v1:
time: 219 us
  Pallas kernels  203 us (93%)
  local copies, waits for them, and re-layouts  12.6 us (6%)
  other arithmetic  2.23 us (1%)
    pallas_call x1, Pallas kernels, final_grads(): pl.pallas_call(functools.partial(ring_kernel, count, parts), in_specs=[an...  139 us
    pallas_call x1, Pallas kernels, project(): pl.pallas_call(functools.partial(gather_kernel, parts), in_specs=[vmem, a...  47 us
    pallas_call x1, Pallas kernels, attention(): pl.pallas_call(functools.partial(attention_kernel, factor), grid=(heads,)...  17.1 us
    unnamed x13, local copies, waits for them, and re-layouts  10.1 us

profile of v1, /device:TPU:0, one launch (start us, length us, event | category | flops | bytes accessed | tf_op | source)
XLA Modules:
  0.0 218.6 jit_solution(10009027616696482074)
XLA Ops:
  0.6 0.9 slice_reduce_fusion.1
  1.5 0.1 pad.3.clone
  1.6 0.1 broadcast_in_dim.22
  1.7 1.5 reverse
  3.2 0.1 slice.19
  3.3 0.6 broadcast_in_dim.23.table_ref
  3.9 47.0 %shard_map.101 = (bf16[768,4096]{1,0:T(8,128)(2,1)}, bf16[768,512]{1,0:T(8,128)(2,1)}, bf16[768,512]{1,0:T(8,128)(2,1)}, bf16[768,512]{1,0:T(8,128)(2,1)}, bf16[2,256,512]{2,1,0:T(8,128)(2,1)}) custom-call(bf16[768,1024]{1,0:T(8,128)(2,1)} %tokens_ref.1, bf16[4096,512]{1,0:T(8,128)(2,1)} %wq_hbm.1, bf16[4096,512]{1,0:T(8,128)(2,1)} %wk_hbm.1, ...), custom_call_target="tpu_custom_call" | custom-call | flops 9663676416 | bytes 150000000 | tf_op jit(solution)/shard_map/pallas_call | solution.py:753
  50.9 17.1 %shard_map.102 = (bf16[768,512]{1,0:T(8,128)(2,1)}, bf16[512,512]{1,0:T(8,128)(2,1)}, bf16[512,512]{1,0:T(8,128)(2,1)}, f32[256,512]{1,0:T(8,128)}, f32[256,512]...) custom-call(s32[1]{0:T(128)} %bitcast.first_ref, bf16[768,512]{1,0:T(8,128)(2,1)} %get-tuple-element.23.q_ref, ...), custom_call_target="tpu_custom_call" | custom-call | flops 1509949440 | bytes 5505024 | tf_op jit(solution)/shard_map/pallas_call | solution.py:135
  68.0 1.3 copy.14
  69.3 139.0 %shard_map.103 = (bf16[768,1024]{1,0:T(8,128)(2,1)}, f32[512,512]{1,0:T(8,128)}, f32[512,512]{1,0:T(8,128)}, f32[512,512]{1,0:T(8,128)}, f32[4,512]{1,0:T(4,128)}) custom-call(bf16[768,4096]{1,0:T(8,128)(2,1)} %get-tuple-element.22.whole_hbm, bf16[768,512]{1,0:T(8,128)(2,1)} %get-tuple-element.27.dq_hbm, bf16[512,512]{1,0:T(8,128)(2,1)} %get-tuple-element.28.dk_hbm, ...), custom_call_target="tpu_custom_call" | custom-call | flops 19327352832 | bytes 400000000 | tf_op jit(solution)/shard_map/pallas_call | solution.py:521
  208.3 0.0 copy-start.1
  208.3 0.0 copy-start
  208.3 0.9 slice_reduce_fusion
  209.2 0.1 copy.11
  209.3 0.7 slice_add_fusion
  210.0 0.8 slice.13
  210.7 0.3 reverse.1
  211.0 0.1 slice.20
  211.1 0.7 pad_maximum_fusion.1
  211.7 2.7 %copy.19 = bf16[768,1024]{1,0:T(8,128)(2,1)} copy(bf16[768,1024]{1,0:T(8,128)(2,1)} %get-tuple-element.44) | data formatting | bytes 3145728
  214.4 2.3 %copy.20 = f32[512,512]{1,0:T(8,128)} copy(f32[512,512]{1,0:T(8,128)} %get-tuple-element.45) | data formatting | bytes 2097152
  216.7 0.0 copy-done.1
  216.7 1.0 copy.21
  217.6 0.0 copy-done
  217.6 1.0 copy.22
  (2 shorter events, 0.0 us)
Async XLA Ops:
  208.3 8.4 %copy-start.1 = (f32[512,512]{1,0:T(8,128)S(1)}, f32[512,512]{1,0:T(8,128)}, u32[]{:S(2)}) copy-start(f32[512,512]{1,0:T(8,128)} %get-tuple-element.46) | copy-start | bytes 3145732
  208.3 9.3 %copy-start = (f32[512,512]{1,0:T(8,128)S(1)}, f32[512,512]{1,0:T(8,128)}, u32[]{:S(2)}) copy-start(f32[512,512]{1,0:T(8,128)} %get-tuple-element.47) | copy-start | bytes 3145732

commit v2 on v0

--- a/solution.py
+++ b/solution.py
@@ -14,13 +14,8 @@
 REACH = PREVIOUS * SEGMENT
 WINDOW = ROWS + REACH
 TABLE = 512
+LANES = 128
 HIDDEN = -1e30
-
-
-def from_behind(value, axis, steps):
-    count = lax.axis_size(axis)
-    leading, last = (max(0, -steps), min(count, count - steps))
-    return lax.ppermute(value, axis, [(source, source + steps) for source in range(leading, last)])
 
 
 def contract_rows(left, right):
@@ -212,38 +207,269 @@
     return jnp.where(place < rows, place * columns, (rows - 1 - above) * columns + column)
 
 
-def ring_kernel(
-    count,
-    whole_ref,
-    dq_ref,
-    dk_ref,
-    dv_ref,
-    line_ref,
-    oq_ref,
-    ok_ref,
-    ov_ref,
-    line_out_ref,
-    sent,
-    got,
-    lines,
-    send_sem,
-    recv_sem,
-    line_send,
-    line_recv,
-):
+def remote(src, dst, send, recv, device):
+    return pltpu.make_async_remote_copy(
+        src_ref=src,
+        dst_ref=dst,
+        send_sem=send,
+        recv_sem=recv,
+        device_id=device,
+        device_id_type=pl.DeviceIdType.MESH,
+    )
+
+
+def meet(count, parts):
     me = lax.axis_index("sp")
-    place = ring_place(me, count)
+    seat = lax.axis_index("tp")
     barrier = pltpu.get_barrier_semaphore()
     for ahead in range(1, count):
         peer = lax.rem(me + ahead, count)
         pl.semaphore_signal(
             barrier, inc=1, device_id={"sp": peer}, device_id_type=pl.DeviceIdType.MESH
         )
-    pl.semaphore_wait(barrier, count - 1)
-
-    grads = (dq_ref, dk_ref, dv_ref)
+    for ahead in range(1, parts):
+        peer = lax.rem(seat + ahead, parts)
+        pl.semaphore_signal(
+            barrier, inc=1, device_id={"tp": peer}, device_id_type=pl.DeviceIdType.MESH
+        )
+    pl.semaphore_wait(barrier, count + parts - 2)
+
+
+def final_loads(hbm, whole, grads, weights, load_sem):
+    whole_hbm, dq_hbm, dk_hbm, dv_hbm, wq_hbm, wk_hbm, wv_hbm = hbm
+    body = whole.shape[0] - REACH
+    return [
+        pltpu.make_async_copy(dq_hbm, grads.at[0], load_sem.at[0]),
+        pltpu.make_async_copy(dk_hbm, grads.at[1, pl.ds(0, body)], load_sem.at[1]),
+        pltpu.make_async_copy(dv_hbm, grads.at[2, pl.ds(0, body)], load_sem.at[2]),
+        pltpu.make_async_copy(whole_hbm, whole, load_sem.at[3]),
+        pltpu.make_async_copy(wq_hbm, weights.at[0], load_sem.at[4]),
+        pltpu.make_async_copy(wk_hbm, weights.at[1], load_sem.at[5]),
+        pltpu.make_async_copy(wv_hbm, weights.at[2], load_sem.at[6]),
+    ]
+
+
+class Halo:
+    def __init__(self, count, grads, tails, back_ref, after, send, recv):
+        self.me = lax.axis_index("sp")
+        self.count = count
+        self.grads, self.tails = grads, tails
+        self.back_ref, self.after, self.sems = back_ref, after, (send, recv)
+
+    def copy(self, which):
+        return remote(
+            self.back_ref.at[which],
+            self.after.at[which],
+            self.sems[0].at[which],
+            self.sems[1].at[which],
+            {"sp": lax.rem(self.me + self.count - 1, self.count)},
+        )
+
+    def start(self):
+        @pl.when(self.me > 0)
+        def _():
+            self.copy(0).start()
+            self.copy(1).start()
+
+    def join(self, which):
+        after = self.after
+
+        @pl.when(self.me < self.count - 1)
+        def _():
+            self.copy(which).wait_recv()
+
+        @pl.when(self.me == self.count - 1)
+        def _():
+            after[which] = jnp.zeros_like(after[which])
+
+        tail = self.tails[which][...] + after[which].astype(jnp.float32)
+        body = self.grads.shape[1] - REACH
+        self.grads[1 + which, body:] = tail.astype(jnp.bfloat16)
+
+    def drain(self):
+        @pl.when(self.me > 0)
+        def _():
+            self.copy(0).wait_send()
+            self.copy(1).wait_send()
+
+
+class Lines:
+    def __init__(self, count, line_ref, out_ref, lines, send, recv):
+        self.me = lax.axis_index("sp")
+        self.count = count
+        self.line_ref, self.out_ref, self.lines = line_ref, out_ref, lines
+        self.sems = (send, recv)
+
+    def copy(self, ahead):
+        return remote(
+            self.line_ref,
+            self.lines.at[ahead - 1],
+            self.sems[0].at[ahead - 1],
+            self.sems[1].at[ahead - 1],
+            {"sp": lax.rem(self.me + ahead, self.count)},
+        )
+
+    def start(self):
+        for ahead in range(1, self.count):
+            self.copy(ahead).start()
+
+    def finish(self):
+        total = self.line_ref[...]
+        for ahead in range(1, self.count):
+            self.copy(ahead).wait()
+            total = total + self.lines[ahead - 1]
+        self.out_ref[...] = total
+
+
+class InputGrad:
+    def __init__(self, parts, grads, weights, input_ref, buffers, sems):
+        self.seat = lax.axis_index("tp")
+        self.core = lax.rem(self.seat, 2)
+        self.row = self.seat // 2
+        self.parts, self.pairs = parts, parts // 2
+        self.grads, self.weights, self.input_ref = grads, weights, input_ref
+        self.pair_sent, self.pair_got, self.cross_sent, self.cross_got, self.kept = buffers
+        self.sems = sems
+        self.block = input_ref.shape[1]
+        self.bands = input_ref.shape[0] // REACH
+        self.units = 2 * self.bands
+
+    def rows(self, band):
+        return pl.ds(pl.multiple_of(band * REACH, REACH), REACH)
+
+    def part(self, band, target):
+        block = pl.ds(pl.multiple_of(target * self.block, self.block), self.block)
+        rows = self.rows(band)
+        term = contract_cols(self.grads[0, rows], self.weights[0, block])
+        term += contract_cols(self.grads[1, rows], self.weights[1, block])
+        return term + contract_cols(self.grads[2, rows], self.weights[2, block])
+
+    def pair_copy(self, band, away):
+        return remote(
+            self.pair_sent.at[band, away],
+            self.pair_got.at[band, away],
+            self.sems[0].at[band, away],
+            self.sems[1].at[band, away],
+            {"tp": self.seat + 1 - 2 * self.core},
+        )
+
+    def cross_copy(self, band, away):
+        return remote(
+            self.cross_sent.at[band, away - 1],
+            self.cross_got.at[band, away - 1],
+            self.sems[2].at[band, away - 1],
+            self.sems[3].at[band, away - 1],
+            {"tp": lax.rem(self.seat + 2 * away, self.parts)},
+        )
+
+    def to_partner(self, band):
+        for away in range(self.pairs):
+            target = 2 * lax.rem(self.row + away, self.pairs) + 1 - self.core
+            self.pair_sent[band, away] = self.part(band, target).astype(jnp.bfloat16)
+            self.pair_copy(band, away).start()
+
+    def across(self, band):
+        for away in range(1, self.pairs):
+            term = self.part(band, lax.rem(self.seat + 2 * away, self.parts))
+            self.pair_copy(band, away).wait_recv()
+            term = term + self.pair_got[band, away].astype(jnp.float32)
+            self.cross_sent[band, away - 1] = term.astype(jnp.bfloat16)
+            self.cross_copy(band, away).start()
+        term = self.part(band, self.seat)
+        self.pair_copy(band, 0).wait_recv()
+        self.kept[band] = term + self.pair_got[band, 0].astype(jnp.float32)
+
+    def finish(self, band):
+        term = self.kept[band]
+        for away in range(1, self.pairs):
+            self.cross_copy(band, away).wait_recv()
+            term = term + self.cross_got[band, away - 1].astype(jnp.float32)
+        self.input_ref[self.rows(band)] = term.astype(jnp.bfloat16)
+
+    def work(self, unit):
+        band = unit // 2
+
+        @pl.when(lax.rem(unit, 2) == 0)
+        def _():
+            self.to_partner(band)
+
+        @pl.when(lax.rem(unit, 2) == 1)
+        def _():
+            self.across(band)
+
+        @pl.when((lax.rem(unit, 2) == 1) & (unit > 2))
+        def _():
+            self.finish(band - 1)
+
+    def drain(self):
+        @pl.loop(0, self.bands)
+        def _(band):
+            for away in range(self.pairs):
+                self.pair_copy(band, away).wait_send()
+            for away in range(1, self.pairs):
+                self.cross_copy(band, away).wait_send()
+
+
+def ring_kernel(
+    count,
+    parts,
+    whole_hbm,
+    dq_hbm,
+    dk_hbm,
+    dv_hbm,
+    wq_hbm,
+    wk_hbm,
+    wv_hbm,
+    dk_tail_ref,
+    dv_tail_ref,
+    back_ref,
+    line_ref,
+    input_ref,
+    oq_ref,
+    ok_ref,
+    ov_ref,
+    line_out_ref,
+    whole,
+    grads,
+    weights,
+    after,
+    lines,
+    pair_sent,
+    pair_got,
+    cross_sent,
+    cross_got,
+    kept,
+    load_sem,
+    back_send,
+    back_recv,
+    line_send,
+    line_recv,
+    pair_send,
+    pair_recv,
+    cross_send,
+    cross_recv,
+    sent,
+    got,
+    send_sem,
+    recv_sem,
+):
+    me = lax.axis_index("sp")
+    place = ring_place(me, count)
+    hbm = (whole_hbm, dq_hbm, dk_hbm, dv_hbm, wq_hbm, wk_hbm, wv_hbm)
+    loads = final_loads(hbm, whole, grads, weights, load_sem)
+    for load in loads:
+        load.start()
+    meet(count, parts)
+    halo = Halo(
+        count, grads, (dk_tail_ref, dv_tail_ref), back_ref, after, back_send, back_recv
+    )
+    shared = Lines(count, line_ref, line_out_ref, lines, line_send, line_recv)
+    buffers = (pair_sent, pair_got, cross_sent, cross_got, kept)
+    sems = (pair_send, pair_recv, cross_send, cross_recv)
+    grad_in = InputGrad(parts, grads, weights, input_ref, buffers, sems)
+
     outs = (oq_ref, ok_ref, ov_ref)
-    half = sent.shape[3]
+    half = got.shape[3]
     onward = (
         ring_index(lax.rem(place + 1, count), count),
         ring_index(lax.rem(place + count - 1, count), count),
@@ -251,96 +477,409 @@
 
     def own(target, side, chain):
         start = pl.multiple_of((2 * ring_index(target, count) + side) * half, half)
-        return contract_rows(whole_ref[:, pl.ds(start, half)], grads[chain][...])
+        return contract_rows(whole[:, pl.ds(start, half)], grads[chain])
 
     def target_of(step, side):
         if side == 0:
             return lax.rem(place - 1 - step + 2 * count, count)
         return lax.rem(place + 1 + step, count)
 
-    def copy_of(step, side, chain):
-        return pltpu.make_async_remote_copy(
-            src_ref=sent.at[side, chain, step],
-            dst_ref=got.at[side, chain, step],
-            send_sem=send_sem.at[side, chain, step],
-            recv_sem=recv_sem.at[side, chain, step],
-            device_id={"sp": onward[side]},
-            device_id_type=pl.DeviceIdType.MESH,
-        )
-
-    def line_copy(ahead):
-        return pltpu.make_async_remote_copy(
-            src_ref=line_ref,
-            dst_ref=lines.at[ahead - 1],
-            send_sem=line_send.at[ahead - 1],
-            recv_sem=line_recv.at[ahead - 1],
-            device_id={"sp": lax.rem(me + ahead, count)},
-            device_id_type=pl.DeviceIdType.MESH,
-        )
+    def copy_of(src, step, side, chain):
+        return remote(
+            src,
+            got.at[side, chain, step],
+            send_sem.at[side, chain, step],
+            recv_sem.at[side, chain, step],
+            {"sp": onward[side]},
+        )
+
+    halo.start()
+    for load in loads:
+        load.wait()
+    for chain in range(3):
+        if chain > 0:
+            halo.join(chain - 1)
+        for side in range(2):
+            sent[side, chain] = own(target_of(0, side), side, chain).astype(jnp.bfloat16)
+            copy_of(sent.at[side, chain], 0, side, chain).start()
+    shared.start()
 
     chains = [(chain, side) for chain in range(3) for side in range(2)]
-    for chain, side in chains:
-        sent[side, chain, 0] = own(target_of(0, side), side, chain).astype(jnp.bfloat16)
-        copy_of(0, side, chain).start()
-    for ahead in range(1, count):
-        line_copy(ahead).start()
 
     @pl.loop(1, count - 1)
     def _(step):
         for chain, side in chains:
-            part = own(target_of(step, side), side, chain)
-            copy_of(step - 1, side, chain).wait_recv()
-            total = part + got[side, chain, step - 1].astype(jnp.float32)
-            sent[side, chain, step] = total.astype(jnp.bfloat16)
-            copy_of(step, side, chain).start()
-
-    total = line_ref[...]
-    for ahead in range(1, count):
-        line_copy(ahead).wait()
-        total = total + lines[ahead - 1]
-    line_out_ref[...] = total
+            part_of = own(target_of(step, side), side, chain)
+            place_of = got.at[side, chain, step - 1]
+            copy_of(sent.at[side, chain], step - 1, side, chain).wait_recv()
+            total = part_of + place_of[...].astype(jnp.float32)
+            place_of[...] = total.astype(jnp.bfloat16)
+            copy_of(place_of, step, side, chain).start()
+            if (chain, side) == (1, 1):
+
+                @pl.when(step <= grad_in.units)
+                def _():
+                    grad_in.work(step - 1)
+
+    for unit in range(min(count - 2, grad_in.units), grad_in.units):
+        grad_in.work(unit)
+    shared.finish()
     for chain, side in chains:
-        part = own(place, side, chain)
-        copy_of(count - 2, side, chain).wait_recv()
-        total = part + got[side, chain, count - 2].astype(jnp.float32)
+        if (chain, side) == (2, 0):
+            grad_in.finish(grad_in.bands - 1)
+        part_of = own(place, side, chain)
+        copy_of(sent.at[side, chain], count - 2, side, chain).wait_recv()
+        total = part_of + got[side, chain, count - 2].astype(jnp.float32)
         outs[chain][side * half : (side + 1) * half] = total
+
+    halo.drain()
 
     @pl.loop(0, count - 1)
     def _(step):
         for chain, side in chains:
-            copy_of(step, side, chain).wait_send()
-
-
-def weight_grads(whole, query_grad, key_grad, value_grad, lines):
+            copy_of(sent.at[side, chain], step, side, chain).wait_send()
+
+    grad_in.drain()
+
+
+def paired(count, parts):
+    return count == 8 and ring_columns(count) == 2 and parts == 4
+
+
+def pair_places(me):
+    level, side = me // 2, lax.rem(me, 2)
+    inner = (level == 1) | (level == 2)
+    near = level // 2
+    made = jnp.where(inner, 1 - near, near)
+    partner = 2 * (level + 1 - 2 * lax.rem(level, 2)) + side
+    return level, side, inner, near, made, partner
+
+
+def pair_kernel(
+    count,
+    parts,
+    whole_hbm,
+    dq_hbm,
+    dk_hbm,
+    dv_hbm,
+    wq_hbm,
+    wk_hbm,
+    wv_hbm,
+    theirs_hbm,
+    dk_tail_ref,
+    dv_tail_ref,
+    back_ref,
+    line_ref,
+    input_ref,
+    oq_ref,
+    ok_ref,
+    ov_ref,
+    line_out_ref,
+    whole,
+    grads,
+    weights,
+    after,
+    lines,
+    pair_sent,
+    pair_got,
+    cross_sent,
+    cross_got,
+    kept,
+    load_sem,
+    back_send,
+    back_recv,
+    line_send,
+    line_recv,
+    pair_send,
+    pair_recv,
+    cross_send,
+    cross_recv,
+    theirs,
+    their_grads,
+    x_sent,
+    x_got,
+    sent,
+    got,
+    result,
+    theirs_sem,
+    swap_send,
+    swap_recv,
+    x_send,
+    x_recv,
+    send_sem,
+    recv_sem,
+    out_sem,
+):
+    me = lax.axis_index("sp")
+    level, side, inner, near, made, partner = pair_places(me)
+    hbm = (whole_hbm, dq_hbm, dk_hbm, dv_hbm, wq_hbm, wk_hbm, wv_hbm)
+    loads = final_loads(hbm, whole, grads, weights, load_sem)
+    loads.insert(4, pltpu.make_async_copy(theirs_hbm, theirs, theirs_sem.at[0]))
+    for load in loads:
+        load.start()
+    meet(count, parts)
+    halo = Halo(
+        count, grads, (dk_tail_ref, dv_tail_ref), back_ref, after, back_send, back_recv
+    )
+    shared = Lines(count, line_ref, line_out_ref, lines, line_send, line_recv)
+    buffers = (pair_sent, pair_got, cross_sent, cross_got, kept)
+    sems = (pair_send, pair_recv, cross_send, cross_recv)
+    grad_in = InputGrad(parts, grads, weights, input_ref, buffers, sems)
+
+    chunks, depth, tile = x_sent.shape[0], x_sent.shape[2], x_sent.shape[3]
+    per = chunks // 3
+    outs = (oq_ref, ok_ref, ov_ref)
+    deep = 2 * (1 + made)
+    rim = 6 * made
+    slot = jnp.where(inner, 0, 1)
+
+    def columns(chunk):
+        return pl.ds(pl.multiple_of(lax.rem(chunk, per) * tile, tile), tile)
+
+    def swap(chunk):
+        return remote(
+            grads.at[chunk // per, :, columns(chunk)],
+            their_grads.at[chunk // per, :, columns(chunk)],
+            swap_send.at[chunk],
+            swap_recv.at[chunk],
+            {"sp": partner},
+        )
+
+    def x_copy(chunk):
+        return remote(
+            x_sent.at[chunk],
+            x_got.at[chunk],
+            x_send.at[chunk],
+            x_recv.at[chunk],
+            {"sp": 2 * level + 1 - side},
+        )
+
+    def deep_copy(chunk):
+        return remote(
+            sent.at[0, chunk],
+            got.at[slot, chunk],
+            send_sem.at[0, chunk],
+            recv_sem.at[slot, chunk],
+            {"sp": deep + side},
+        )
+
+    def rim_copy(chunk):
+        return remote(
+            sent.at[1, chunk],
+            got.at[0, chunk],
+            send_sem.at[1, chunk],
+            recv_sem.at[0, chunk],
+            {"sp": rim + side},
+        )
+
+    def arrived(chunk, which):
+        return remote(
+            sent.at[0, chunk],
+            got.at[which, chunk],
+            send_sem.at[0, chunk],
+            recv_sem.at[which, chunk],
+            {"sp": deep + side},
+        )
+
+    def sums(target, chunk):
+        start = pl.multiple_of(target * depth, depth)
+        mine = whole[:, pl.ds(start, depth)]
+        start = pl.multiple_of((target - made * (count // 2)) * depth, depth)
+        their = theirs[:, pl.ds(start, depth)]
+        term = contract_rows(mine, grads[chunk // per, :, columns(chunk)])
+        return term + contract_rows(their, their_grads[chunk // per, :, columns(chunk)])
+
+    def halve(chunk):
+        swap(chunk).wait_recv()
+        x_sent[chunk, 0] = sums(deep + 1 - side, chunk).astype(jnp.bfloat16)
+        x_sent[chunk, 1] = sums(rim + 1 - side, chunk).astype(jnp.bfloat16)
+        x_copy(chunk).start()
+
+    def onward(chunk):
+        term = sums(deep + side, chunk)
+        x_copy(chunk).wait_recv()
+        term = term + x_got[chunk, 0].astype(jnp.float32)
+        sent[0, chunk] = term.astype(jnp.bfloat16)
+        deep_copy(chunk).start()
+        term = sums(rim + side, chunk) + x_got[chunk, 1].astype(jnp.float32)
+
+        @pl.when(inner)
+        def _():
+            sent[1, chunk] = term.astype(jnp.bfloat16)
+            rim_copy(chunk).start()
+
+        @pl.when(jnp.logical_not(inner))
+        def _():
+            result[chunk // per, :, columns(chunk)] = term
+
+    def store(chunk, matrix):
+        return pltpu.make_async_copy(
+            result.at[matrix, :, columns(chunk)],
+            outs[matrix].at[:, columns(chunk)],
+            out_sem.at[chunk],
+        )
+
+    def finish(chunk):
+        arrived(chunk, 0).wait_recv()
+        term = got[0, chunk].astype(jnp.float32)
+
+        @pl.when(inner)
+        def _():
+            arrived(chunk, 1).wait_recv()
+            total = term + got[1, chunk].astype(jnp.float32)
+            result[chunk // per, :, columns(chunk)] = total
+
+        @pl.when(jnp.logical_not(inner))
+        def _():
+            total = term + result[chunk // per, :, columns(chunk)]
+            result[chunk // per, :, columns(chunk)] = total
+
+        for matrix in range(3):
+
+            @pl.when(chunk // per == matrix)
+            def _():
+                store(chunk, matrix).start()
+
+    halo.start()
+    loads[0].wait()
+    for chunk in range(per):
+        swap(chunk).start()
+    for which in range(2):
+        loads[1 + which].wait()
+        halo.join(which)
+        for chunk in range(per):
+            swap((1 + which) * per + chunk).start()
+    for load in loads[3:]:
+        load.wait()
+    shared.start()
+
+    lag = 3
+
+    @pl.loop(0, chunks + lag)
+    def _(step):
+        @pl.when(step < chunks)
+        def _():
+            halve(step)
+
+        @pl.when((step > 0) & (step <= chunks))
+        def _():
+            onward(step - 1)
+
+        @pl.when(step >= lag)
+        def _():
+            finish(step - lag)
+
+        unit = (step - 1) // 2
+
+        @pl.when((lax.rem(step, 2) == 1) & (unit < grad_in.units))
+        def _():
+            grad_in.work(unit)
+
+    for unit in range(min((chunks + lag) // 2, grad_in.units), grad_in.units):
+        grad_in.work(unit)
+    shared.finish()
+    grad_in.finish(grad_in.bands - 1)
+    halo.drain()
+
+    @pl.loop(0, chunks)
+    def _(chunk):
+        swap(chunk).wait_send()
+        x_copy(chunk).wait_send()
+        deep_copy(chunk).wait_send()
+        store(chunk, 0).wait()
+
+        @pl.when(inner)
+        def _():
+            rim_copy(chunk).wait_send()
+
+    grad_in.drain()
+
+
+def final_grads(whole, theirs, grads, tails, back, lines, weights):
     count = lax.axis_size("sp")
-    features = whole.shape[1]
-    width = query_grad.shape[1]
-    half = features // count // 2
+    parts = lax.axis_size("tp")
+    pairs = parts // 2
+    length, features = whole.shape
+    width = weights[0].shape[1]
+    depth = features // count
+    block = features // parts
+    bands = length // REACH
     vmem = pl.BlockSpec(memory_space=pltpu.VMEM)
-    out = jax.ShapeDtypeStruct((2 * half, width), jnp.float32)
+    anywhere = pl.BlockSpec(memory_space=pl.ANY)
+    out = jax.ShapeDtypeStruct((depth, width), jnp.float32)
+    dma = pltpu.SemaphoreType.DMA
+    low = jnp.bfloat16
+    pair = paired(count, parts)
+    scratch = [
+        pltpu.VMEM((length, features), low),
+        pltpu.VMEM((3, length, width), low),
+        pltpu.VMEM((3, features, width), low),
+        pltpu.VMEM((2, REACH, width), low),
+        pltpu.VMEM((count - 1,) + lines.shape, jnp.float32),
+        pltpu.VMEM((bands, pairs, REACH, block), low),
+        pltpu.VMEM((bands, pairs, REACH, block), low),
+        pltpu.VMEM((bands, pairs - 1, REACH, block), low),
+        pltpu.VMEM((bands, pairs - 1, REACH, block), low),
+        pltpu.VMEM((bands, REACH, block), jnp.float32),
+        dma((7,)),
+        dma((2,)),
+        dma((2,)),
+        dma((count - 1,)),
+        dma((count - 1,)),
+        dma((bands, pairs)),
+        dma((bands, pairs)),
+        dma((bands, pairs - 1)),
+        dma((bands, pairs - 1)),
+    ]
+    if pair:
+        tile = min(width, LANES)
+        chunks = 3 * width // tile
+        scratch += [
+            pltpu.VMEM((length, features // 2), low),
+            pltpu.VMEM((3, length, width), low),
+            pltpu.VMEM((chunks, 2, depth, tile), low),
+            pltpu.VMEM((chunks, 2, depth, tile), low),
+            pltpu.VMEM((2, chunks, depth, tile), low),
+            pltpu.VMEM((2, chunks, depth, tile), low),
+            pltpu.VMEM((3, depth, width), jnp.float32),
+            dma((1,)),
+            dma((chunks,)),
+            dma((chunks,)),
+            dma((chunks,)),
+            dma((chunks,)),
+            dma((2, chunks)),
+            dma((2, chunks)),
+            dma((chunks,)),
+        ]
+    else:
+        scratch += [
+            pltpu.VMEM((2, 3, depth // 2, width), low),
+            pltpu.VMEM((2, 3, count - 1, depth // 2, width), low),
+            dma((2, 3, count - 1)),
+            dma((2, 3, count - 1)),
+        ]
+    place = anywhere if pair else vmem
     return pl.pallas_call(
-        functools.partial(ring_kernel, count),
-        in_specs=[vmem] * 5,
-        out_specs=[vmem] * 4,
-        out_shape=[out, out, out, jax.ShapeDtypeStruct(lines.shape, jnp.float32)],
-        scratch_shapes=[
-            pltpu.VMEM((2, 3, count - 1, half, width), jnp.bfloat16),
-            pltpu.VMEM((2, 3, count - 1, half, width), jnp.bfloat16),
-            pltpu.VMEM((count - 1,) + lines.shape, jnp.float32),
-            pltpu.SemaphoreType.DMA((2, 3, count - 1)),
-            pltpu.SemaphoreType.DMA((2, 3, count - 1)),
-            pltpu.SemaphoreType.DMA((count - 1,)),
-            pltpu.SemaphoreType.DMA((count - 1,)),
+        functools.partial(pair_kernel if pair else ring_kernel, count, parts),
+        in_specs=[anywhere] * (7 + pair) + [vmem] * 4,
+        out_specs=[vmem] + [place] * 3 + [vmem],
+        out_shape=[
+            jax.ShapeDtypeStruct((length, block), low),
+            out,
+            out,
+            out,
+            jax.ShapeDtypeStruct(lines.shape, jnp.float32),
         ],
+        scratch_shapes=scratch,
         compiler_params=pltpu.CompilerParams(
-            collective_id=0, has_side_effects=True, vmem_limit_bytes=56 * 1024 * 1024
+            collective_id=0, has_side_effects=True, vmem_limit_bytes=63 * 1024 * 1024
         ),
         cost_estimate=pl.CostEstimate(
-            flops=6 * whole.shape[0] * features * width,
+            flops=12 * length * features * width,
             bytes_accessed=400_000_000,
             transcendentals=0,
         ),
-    )(whole, query_grad, key_grad, value_grad, lines)
+    )(whole, *grads, *weights, *theirs, *tails, back, lines)
 
 
 def gather_kernel(
@@ -354,6 +893,7 @@
     k_ref,
     v_ref,
     prev_ref,
+    theirs_ref,
     held,
     weights,
     total,
@@ -369,6 +909,7 @@
     halo_recv,
     load_sem,
     store_sem,
+    *ship_refs,
 ):
     me = lax.axis_index("tp")
     seat = lax.axis_index("sp")
@@ -412,20 +953,16 @@
         pl.semaphore_signal(
             barrier, inc=1, device_id={"sp": other}, device_id_type=pl.DeviceIdType.MESH
         )
-    pl.semaphore_wait(barrier, parts + 1)
+    ship = len(ship_refs) > 0
+    if ship:
+        level, lane, inner, near, made, mate = pair_places(seat)
+        pl.semaphore_signal(
+            barrier, inc=1, device_id={"sp": mate}, device_id_type=pl.DeviceIdType.MESH
+        )
+    pl.semaphore_wait(barrier, parts + 1 + ship)
 
     def rows(chunk):
         return pl.ds(chunk * REACH, REACH)
-
-    def remote(src, dst, send, recv, device):
-        return pltpu.make_async_remote_copy(
-            src_ref=src,
-            dst_ref=dst,
-            send_sem=send,
-            recv_sem=recv,
-            device_id=device,
-            device_id_type=pl.DeviceIdType.MESH,
-        )
 
     def far(chunk, away):
         return remote(
@@ -473,11 +1010,46 @@
             else:
                 total[matrix, chunk] += term
 
+    if ship:
+        ship_got, ship_send, ship_recv, pass_send, pass_recv, keep_sem = ship_refs
+        core = lax.rem(me, 2)
+        shipped = jnp.where(inner, near, 1 - near)
+        ready = me // 2 == shipped
+
+        def ship_copy(chunk, src):
+            return remote(
+                src,
+                ship_got.at[chunk, core],
+                ship_send.at[chunk],
+                ship_recv.at[chunk],
+                {"sp": mate},
+            )
+
+        def pass_on(chunk):
+            place = ship_got.at[chunk, core]
+            return remote(
+                place, place, pass_send.at[chunk], pass_recv.at[chunk], {"tp": partner}
+            )
+
+        def keep(chunk, which):
+            start = pl.multiple_of(which * block, block)
+            return pltpu.make_async_copy(
+                ship_got.at[chunk, which],
+                theirs_ref.at[rows(chunk), pl.ds(start, block)],
+                keep_sem.at[chunk, which],
+            )
+
     backwards = list(range(chunks))[::-1]
     for chunk in backwards:
         for away in range(1, pairs):
             far(chunk, away).start()
         side(chunk).start()
+        if ship:
+
+            @pl.when(ready)
+            def _():
+                ship_copy(chunk, tokens_ref.at[rows(chunk)]).start()
+
     for slot in range(2):
         for matrix in range(3):
             load(slot, matrix).wait()
@@ -495,6 +1067,12 @@
         for away in range(1, pairs):
             far(chunk, away).wait_recv()
             relay(chunk, away).start()
+            if ship:
+
+                @pl.when(jnp.logical_not(ready))
+                def _():
+                    ship_copy(chunk, held.at[chunk, source(me, 1)]).start()
+
             store(chunk, 2 * away).start()
             add(chunk, 2 * away, held[chunk, source(me, away)])
         for away in range(1, pairs):
@@ -507,8 +1085,24 @@
             halo[0] = total[1, chunk].astype(jnp.bfloat16)
             halo[1] = total[2, chunk].astype(jnp.bfloat16)
             neighbour().start()
+        if ship and chunk + 1 < chunks:
+            ship_copy(chunk + 1, tokens_ref.at[rows(chunk)]).wait_recv()
+            pass_on(chunk + 1).start()
+            keep(chunk + 1, core).start()
     neighbour().wait()
     prev_ref[...] = halo_got[...]
+    if ship:
+        ship_copy(0, tokens_ref.at[rows(0)]).wait_recv()
+        pass_on(0).start()
+        keep(0, core).start()
+        for chunk in backwards:
+            pass_on(chunk).wait_recv()
+            keep(chunk, 1 - core).start()
+        for chunk in backwards:
+            ship_copy(chunk, tokens_ref.at[rows(chunk)]).wait_send()
+            pass_on(chunk).wait_send()
+            keep(chunk, core).wait()
+            keep(chunk, 1 - core).wait()
     for chunk in backwards:
         side(chunk).wait_send()
         for away in range(1, pairs):
@@ -528,16 +1122,28 @@
     anywhere = pl.BlockSpec(memory_space=pl.ANY)
     narrow = jax.ShapeDtypeStruct((length, width), jnp.bfloat16)
     dma = pltpu.SemaphoreType.DMA
+    ship = paired(lax.axis_size("sp"), parts)
+    extra = []
+    if ship:
+        extra = [
+            pltpu.VMEM((chunks, 2, REACH, block), jnp.bfloat16),
+            dma((chunks,)),
+            dma((chunks,)),
+            dma((chunks,)),
+            dma((chunks,)),
+            dma((chunks, 2)),
+        ]
     return pl.pallas_call(
         functools.partial(gather_kernel, parts),
         in_specs=[vmem, anywhere, anywhere, anywhere],
-        out_specs=[anywhere, vmem, vmem, vmem, vmem],
+        out_specs=[anywhere, vmem, vmem, vmem, vmem, anywhere],
         out_shape=[
             jax.ShapeDtypeStruct((length, block * parts), jnp.bfloat16),
             narrow,
             narrow,
             narrow,
             jax.ShapeDtypeStruct((2, REACH, width), jnp.bfloat16),
+            jax.ShapeDtypeStruct((length, 2 * block) if ship else (8, LANES), jnp.bfloat16),
         ],
         scratch_shapes=[
             pltpu.VMEM((chunks, parts, REACH, block), jnp.bfloat16),
@@ -555,7 +1161,8 @@
             dma(()),
             dma((parts, 3)),
             dma((chunks, parts)),
-        ],
+        ]
+        + extra,
         compiler_params=pltpu.CompilerParams(
             collective_id=1, has_side_effects=True, vmem_limit_bytes=56 * 1024 * 1024
         ),
@@ -566,20 +1173,20 @@
 
 
 def shards(tokens, query_weight, key_weight, value_weight, position_bias, out_grad):
-    weights = jnp.concatenate([query_weight, key_weight, value_weight], axis=1)
-    whole, query, keys, values, prev = project(tokens, query_weight, key_weight, value_weight)
+    whole, query, keys, values, prev, theirs = project(
+        tokens, query_weight, key_weight, value_weight
+    )
     query_grad, key_body, value_body, key_tail, value_tail, back, lines = attention(
         query, keys, values, prev, out_grad, position_bias
     )
-    after = from_behind(back, "sp", -1)
-    key_grad = jnp.concatenate([key_body, (key_tail + after[0]).astype(jnp.bfloat16)])
-    value_grad = jnp.concatenate([value_body, (value_tail + after[1]).astype(jnp.bfloat16)])
-    grads = jnp.concatenate([query_grad, key_grad, value_grad], axis=1)
-    input_part = contract_cols(grads, weights).astype(jnp.bfloat16)
-    input_grad = lax.psum_scatter(input_part, "tp", scatter_dimension=1, tiled=True)
-    barrier = lax.optimization_barrier((key_grad, input_part))
-    query_weight_grad, key_weight_grad, value_weight_grad, lines = weight_grads(
-        whole, query_grad, barrier[0], value_grad, lines[:, 0]
+    input_grad, query_weight_grad, key_weight_grad, value_weight_grad, lines = final_grads(
+        whole,
+        (theirs,) if paired(lax.axis_size("sp"), lax.axis_size("tp")) else (),
+        (query_grad, key_body, value_body),
+        (key_tail, value_tail),
+        back,
+        lines[:, 0],
+        (query_weight, key_weight, value_weight),
     )
     bias_grad = table_to_bias(lines, position_bias.shape[1])
     return input_grad, query_weight_grad, key_weight_grad, value_weight_grad, bias_grad

time: 257 us -> 235 us (0.914)
  Pallas kernels: 195 us -> 219 us
  waiting for transfers between devices: 15.4 us -> 0 us
  matrix products: 15.2 us -> 0 us
  between operations: 14.1 us -> 0.69 us
    ppermute x1 -> x0, waiting for transfers between devices: 15.3 us -> none  [from_behind(): lax.ppermute(value, axis, [(source, source + steps) for source in range(l...]
    dot_general x1 -> x0, matrix products: 15.2 us -> none  [contract_cols(): lax.dot_general(left, right, (((1,), (1,)), ((), ())), preferred_element_...]
    pallas_call x1, Pallas kernels: 130 us -> 143 us  [final_grads(): pl.pallas_call(functools.partial(pair_kernel if pair else ring_kernel, co...]
    pallas_call x1, Pallas kernels: 47 us -> 58.8 us  [project(): pl.pallas_call(functools.partial(gather_kernel, parts), in_specs=[vmem, a...]
    unnamed x16 -> x13, local copies, waits for them, and re-layouts: 8.72 us -> 10.1 us
  transfers between devices with their start and end apart: 2 -> 0, of which waited for: 1 -> 0; matrix products, arithmetic and copies ran while one was open for 2% -> 0% of each run, Pallas kernels for 51% -> 0%
where the time goes in v2:
time: 235 us
  Pallas kernels  219 us (93%)
  local copies, waits for them, and re-layouts  12.6 us (5%)
    pallas_call x1, Pallas kernels, final_grads(): pl.pallas_call(functools.partial(pair_kernel if pair else ring_kernel, co...  143 us
    pallas_call x1, Pallas kernels, project(): pl.pallas_call(functools.partial(gather_kernel, parts), in_specs=[vmem, a...  58.8 us
    pallas_call x1, Pallas kernels, attention(): pl.pallas_call(functools.partial(attention_kernel, factor), grid=(heads,)...  17.1 us
    unnamed x13, local copies, waits for them, and re-layouts  10.1 us

profile of v2, /device:TPU:0, one launch (start us, length us, event | category | flops | bytes accessed | tf_op | source)
XLA Modules:
  0.0 234.6 jit_solution(10588841858210316090)
XLA Ops:
  0.6 0.9 slice_reduce_fusion.1
  1.5 0.1 pad.3.clone
  1.6 0.1 broadcast_in_dim.22
  1.7 1.5 reverse
  3.2 0.1 slice.19
  3.3 0.6 broadcast_in_dim.23.table_ref
  3.9 58.8 %shard_map.101 = (bf16[768,4096]{1,0:T(8,128)(2,1)}, bf16[768,512]{1,0:T(8,128)(2,1)}, bf16[768,512]{1,0:T(8,128)(2,1)}, bf16[768,512]{1,0:T(8,128)(2,1)}, bf16[...) custom-call(bf16[768,1024]{1,0:T(8,128)(2,1)} %tokens_ref.1, bf16[4096,512]{1,0:T(8,128)(2,1)} %wq_hbm.1, ...), custom_call_target="tpu_custom_call" | custom-call | flops 9663676416 | bytes 150000000 | tf_op jit(solution)/shard_map/pallas_call | solution.py:1136
  62.7 17.1 %shard_map.102 = (bf16[768,512]{1,0:T(8,128)(2,1)}, bf16[512,512]{1,0:T(8,128)(2,1)}, bf16[512,512]{1,0:T(8,128)(2,1)}, f32[256,512]{1,0:T(8,128)}, f32[256,512]...) custom-call(s32[1]{0:T(128)} %bitcast.first_ref, bf16[768,512]{1,0:T(8,128)(2,1)} %get-tuple-element.24.q_ref, ...), custom_call_target="tpu_custom_call" | custom-call | flops 1509949440 | bytes 5505024 | tf_op jit(solution)/shard_map/pallas_call | solution.py:136
  79.8 1.3 copy.14
  81.1 143.2 %shard_map.103 = (bf16[768,1024]{1,0:T(8,128)(2,1)}, f32[512,512]{1,0:T(8,128)}, f32[512,512]{1,0:T(8,128)}, f32[512,512]{1,0:T(8,128)}, f32[4,512]{1,0:T(4,128)}) custom-call(bf16[768,4096]{1,0:T(8,128)(2,1)} %get-tuple-element.23.whole_hbm, bf16[768,512]{1,0:T(8,128)(2,1)} %get-tuple-element.28.dq_hbm, bf16[512,512]{1,0:T(8,128)(2,1)} %get-tuple-element.29.dk_hbm, ...), custom_call_target="tpu_custom_call" | custom-call | flops 19327352832 | bytes 400000000 | tf_op jit(solution)/shard_map/pallas_call | solution.py:862
  224.3 0.0 copy-start.1
  224.3 0.0 copy-start
  224.3 0.9 slice_reduce_fusion
  225.2 0.1 copy.11
  225.3 0.7 slice_add_fusion
  226.0 0.8 slice.13
  226.7 0.3 reverse.1
  227.0 0.1 slice.20
  227.1 0.7 pad_maximum_fusion.1
  227.7 2.7 %copy.19 = bf16[768,1024]{1,0:T(8,128)(2,1)} copy(bf16[768,1024]{1,0:T(8,128)(2,1)} %get-tuple-element.46) | data formatting | bytes 3145728
  230.4 2.3 copy.20
  232.7 0.0 copy-done.1
  232.7 1.0 copy.21
  233.7 0.0 copy-done
  233.7 1.0 copy.22
  (2 shorter events, 0.0 us)
Async XLA Ops:
  224.3 8.4 %copy-start.1 = (f32[512,512]{1,0:T(8,128)S(1)}, f32[512,512]{1,0:T(8,128)}, u32[]{:S(2)}) copy-start(f32[512,512]{1,0:T(8,128)} %get-tuple-element.48) | copy-start | bytes 3145732
  224.3 9.4 %copy-start = (f32[512,512]{1,0:T(8,128)S(1)}, f32[512,512]{1,0:T(8,128)}, u32[]{:S(2)}) copy-start(f32[512,512]{1,0:T(8,128)} %get-tuple-element.49) | copy-start | bytes 3145732

commit v3 on v2

--- a/solution.py
+++ b/solution.py
@@ -15,6 +15,7 @@
 WINDOW = ROWS + REACH
 TABLE = 512
 LANES = 128
+GRAIN = 256
 HIDDEN = -1e30
 
 
@@ -41,145 +42,87 @@
     return jnp.sum(tile, axis=0, keepdims=True)
 
 
-def attention_kernel(
-    factor,
-    first_ref,
-    q_ref,
-    k_ref,
-    v_ref,
-    prev_ref,
-    g_ref,
-    table_ref,
-    dq_ref,
-    dk_ref,
-    dv_ref,
-    dk_tail_ref,
-    dv_tail_ref,
-    back_ref,
-    table_grad_ref,
-    k_all,
-    v_all,
-    dk_all,
-    dv_all,
-):
-    length = q_ref.shape[0]
-    k_all[:REACH] = prev_ref[0]
-    k_all[REACH:] = k_ref[...]
-    v_all[:REACH] = prev_ref[1]
-    v_all[REACH:] = v_ref[...]
-    dk_all[...] = jnp.zeros_like(dk_all)
-    dv_all[...] = jnp.zeros_like(dv_all)
-    first = first_ref[0]
-    table = jnp.broadcast_to(table_ref[0], (ROWS, TABLE))
-    bias = pltpu.roll(table, 0, 1, stride=1, stride_axis=0)[:, :WINDOW]
-    row = lax.broadcasted_iota(jnp.int32, (ROWS, WINDOW), 0) // SEGMENT
-    column = lax.broadcasted_iota(jnp.int32, (ROWS, WINDOW), 1)
-    behind = column // SEGMENT - row
-    bias = jnp.where((behind >= 0) & (behind <= PREVIOUS), bias, HIDDEN)
-    bias_sum = jnp.zeros((ROWS, WINDOW), jnp.float32)
-    for start in range(0, length, ROWS):
-        q = q_ref[start : start + ROWS]
-        g = g_ref[start : start + ROWS]
-        k = k_all[start : start + WINDOW]
-        v = v_all[start : start + WINDOW]
-        mask = bias
-        if start < REACH:
-            mask = jnp.where(column + start < first, HIDDEN, bias)
-        scores = contract_cols(q, k) * factor + mask
-        top = jnp.max(scores, axis=1, keepdims=True)
-        raised = jnp.exp(scores - top)
-        weights = raised * (1.0 / jnp.sum(raised, axis=1, keepdims=True))
-        prob_grad = contract_cols(g, v)
-        delta = jnp.sum(weights * prob_grad, axis=1, keepdims=True)
-        score_grad = weights * (prob_grad - delta)
-        bias_sum = bias_sum + score_grad
-        low = score_grad.astype(jnp.bfloat16)
-        dq = jnp.dot(low, k, preferred_element_type=jnp.float32) * factor
-        dq_ref[start : start + ROWS] = dq.astype(jnp.bfloat16)
-        dk_all[start : start + WINDOW] += contract_rows(low, q)
-        dv_all[start : start + WINDOW] += contract_rows(weights.astype(jnp.bfloat16), g)
-    back_ref[0] = (dk_all[:REACH] * factor).astype(jnp.bfloat16)
-    back_ref[1] = dv_all[:REACH].astype(jnp.bfloat16)
-    dk_ref[...] = (dk_all[REACH:length] * factor).astype(jnp.bfloat16)
-    dv_ref[...] = dv_all[REACH:length].astype(jnp.bfloat16)
-    dk_tail_ref[...] = dk_all[length:] * factor
-    dv_tail_ref[...] = dv_all[length:]
-    padded = jnp.concatenate([bias_sum, jnp.zeros((ROWS, TABLE - WINDOW), jnp.float32)], axis=1)
-    table_grad_ref[0] = diagonal_sums(padded)
-
-
-def attention(query, keys, values, prev, out_grad, position_bias):
-    length, width = query.shape
-    heads, entries = position_bias.shape
-    head = width // heads
-    factor = head ** (-0.5)
-    table = jnp.concatenate(
-        [
-            position_bias[:, ::-1],
-            jnp.zeros((heads, WINDOW - entries), jnp.float32),
-            jnp.broadcast_to(position_bias[:, entries - 1 :], (heads, TABLE - WINDOW)),
-        ],
-        axis=1,
-    )[:, None]
-    first = jnp.where(lax.axis_index("sp") == 0, REACH, 0).astype(jnp.int32)[None]
-
-    def rows(count):
-        return pl.BlockSpec((count, head), lambda h: (0, h))
-
-    line = pl.BlockSpec((1, 1, TABLE), lambda h: (h, 0, 0))
-
-    def shape(count, kind):
-        return jax.ShapeDtypeStruct((count, width), kind)
-
-    body = length - REACH
-    elements = heads * length * WINDOW
-    outs = pl.pallas_call(
-        functools.partial(attention_kernel, factor),
-        grid=(heads,),
-        in_specs=[
-            pl.BlockSpec(memory_space=pltpu.SMEM),
-            rows(length),
-            rows(length),
-            rows(length),
-            pl.BlockSpec((2, REACH, head), lambda h: (0, 0, h)),
-            rows(length),
-            line,
-        ],
-        out_specs=[
-            rows(length),
-            rows(body),
-            rows(body),
-            rows(REACH),
-            rows(REACH),
-            pl.BlockSpec((2, REACH, head), lambda h: (0, 0, h)),
-            line,
-        ],
-        out_shape=[
-            shape(length, jnp.bfloat16),
-            shape(body, jnp.bfloat16),
-            shape(body, jnp.bfloat16),
-            shape(REACH, jnp.float32),
-            shape(REACH, jnp.float32),
-            jax.ShapeDtypeStruct((2, REACH, width), jnp.bfloat16),
-            jax.ShapeDtypeStruct((heads, 1, TABLE), jnp.float32),
-        ],
-        scratch_shapes=[
-            pltpu.VMEM((length + REACH, head), jnp.bfloat16),
-            pltpu.VMEM((length + REACH, head), jnp.bfloat16),
-            pltpu.VMEM((length + REACH, head), jnp.float32),
-            pltpu.VMEM((length + REACH, head), jnp.float32),
-        ],
-        cost_estimate=pl.CostEstimate(
-            flops=10 * elements * head, bytes_accessed=14 * length * width, transcendentals=elements
-        ),
-    )(first, query, keys, values, prev, out_grad, table)
-    return outs
-
-
-def table_to_bias(summed, entries):
-    near = summed[:, 1:entries][:, ::-1]
-    far = summed[:, :1] + jnp.sum(summed[:, WINDOW:], axis=1, keepdims=True)
-    return jnp.concatenate([near, far], axis=1)
+def table_map(entries):
+    entry = lax.broadcasted_iota(jnp.int32, (entries, TABLE), 0)
+    column = lax.broadcasted_iota(jnp.int32, (entries, TABLE), 1)
+    near = column + entry == entries - 1
+    far = (column >= WINDOW) & (entry == entries - 1)
+    return jnp.where(near | far, 1.0, 0.0).astype(jnp.float32)
+
+
+def exact(left, right, axis):
+    return lax.dot_general(
+        left,
+        right,
+        (((1,), (axis,)), ((), ())),
+        precision=lax.Precision.HIGHEST,
+        preferred_element_type=jnp.float32,
+    )
+
+
+class Attention:
+    def __init__(self, factor, heads, q_all, k_all, v_all, g_ref, dq_ref, scratch):
+        self.factor, self.heads = factor, heads
+        self.q_all, self.k_all, self.v_all = q_all, k_all, v_all
+        self.g_ref, self.dq_ref = g_ref, dq_ref
+        self.bias_all, self.bias_sum, self.dk_all, self.dv_all = scratch
+        self.head = q_all.shape[1] // heads
+
+    def begin(self, table_rows):
+        self.dk_all[...] = jnp.zeros_like(self.dk_all)
+        self.dv_all[...] = jnp.zeros_like(self.dv_all)
+        self.bias_sum[...] = jnp.zeros_like(self.bias_sum)
+        row = lax.broadcasted_iota(jnp.int32, (ROWS, WINDOW), 0) // SEGMENT
+        column = lax.broadcasted_iota(jnp.int32, (ROWS, WINDOW), 1)
+        behind = column // SEGMENT - row
+        seen = (behind >= 0) & (behind <= PREVIOUS)
+        for head in range(self.heads):
+            table = jnp.broadcast_to(table_rows[head : head + 1], (ROWS, TABLE))
+            bias = pltpu.roll(table, 0, 1, stride=1, stride_axis=0)[:, :WINDOW]
+            self.bias_all[head] = jnp.where(seen, bias, HIDDEN)
+
+    def attend(self, start):
+        @pl.loop(0, self.heads)
+        def _(head):
+            columns = pl.ds(pl.multiple_of(head * self.head, self.head), self.head)
+            rows = slice(start, start + ROWS)
+            window = slice(start, start + WINDOW)
+            q = self.q_all[rows, columns]
+            g = self.g_ref[rows, columns]
+            k = self.k_all[window, columns]
+            v = self.v_all[window, columns]
+            mask = self.bias_all[head]
+            if start < REACH:
+                first = jnp.where(lax.axis_index("sp") == 0, REACH - start, 0)
+                column = lax.broadcasted_iota(jnp.int32, (ROWS, WINDOW), 1)
+                mask = jnp.where(column < first, HIDDEN, mask)
+            scores = contract_cols(q, k) * self.factor + mask
+            top = jnp.max(scores, axis=1, keepdims=True)
+            raised = jnp.exp(scores - top)
+            weights = raised * (1.0 / jnp.sum(raised, axis=1, keepdims=True))
+            prob_grad = contract_cols(g, v)
+            delta = jnp.sum(weights * prob_grad, axis=1, keepdims=True)
+            score_grad = weights * (prob_grad - delta)
+            self.bias_sum[head] += score_grad
+            low = score_grad.astype(jnp.bfloat16)
+            dq = jnp.dot(low, k, preferred_element_type=jnp.float32) * self.factor
+            self.dq_ref[rows, columns] = dq.astype(jnp.bfloat16)
+            self.dk_all[window, columns] += contract_rows(low, q)
+            self.dv_all[window, columns] += contract_rows(weights.astype(jnp.bfloat16), g)
+
+    def end(self, dk_ref, dv_ref, dk_tail_ref, dv_tail_ref, back_ref, line_ref):
+        length = self.q_all.shape[0]
+        dk_all, dv_all, factor = self.dk_all, self.dv_all, self.factor
+        back_ref[0] = (dk_all[:REACH] * factor).astype(jnp.bfloat16)
+        back_ref[1] = dv_all[:REACH].astype(jnp.bfloat16)
+        dk_ref[...] = (dk_all[REACH:length] * factor).astype(jnp.bfloat16)
+        dv_ref[...] = dv_all[REACH:length].astype(jnp.bfloat16)
+        dk_tail_ref[...] = dk_all[length:] * factor
+        dv_tail_ref[...] = dv_all[length:]
+        for head in range(self.heads):
+            blank = jnp.zeros((ROWS, TABLE - WINDOW), jnp.float32)
+            padded = jnp.concatenate([self.bias_sum[head], blank], axis=1)
+            line_ref[head : head + 1] = diagonal_sums(padded)
 
 
 def ring_columns(count):
@@ -318,7 +261,7 @@
         for ahead in range(1, self.count):
             self.copy(ahead).wait()
             total = total + self.lines[ahead - 1]
-        self.out_ref[...] = total
+        self.out_ref[...] = exact(total, table_map(self.out_ref.shape[1]), 1)
 
 
 class InputGrad:
@@ -753,7 +696,7 @@
         load.wait()
     shared.start()
 
-    lag = 3
+    lag = 3 * chunks // 4
 
     @pl.loop(0, chunks + lag)
     def _(step):
@@ -795,7 +738,7 @@
     grad_in.drain()
 
 
-def final_grads(whole, theirs, grads, tails, back, lines, weights):
+def final_grads(whole, theirs, grads, tails, back, lines, weights, entries):
     count = lax.axis_size("sp")
     parts = lax.axis_size("tp")
     pairs = parts // 2
@@ -868,7 +811,7 @@
             out,
             out,
             out,
-            jax.ShapeDtypeStruct(lines.shape, jnp.float32),
+            jax.ShapeDtypeStruct((lines.shape[0], entries), jnp.float32),
         ],
         scratch_shapes=scratch,
         compiler_params=pltpu.CompilerParams(
@@ -888,17 +831,29 @@
     wq_ref,
     wk_ref,
     wv_ref,
+    g_ref,
+    bias_ref,
     whole_ref,
-    q_ref,
-    k_ref,
-    v_ref,
-    prev_ref,
     theirs_ref,
+    dq_ref,
+    dk_ref,
+    dv_ref,
+    dk_tail_ref,
+    dv_tail_ref,
+    back_ref,
+    line_ref,
     held,
     weights,
     total,
     halo,
     halo_got,
+    q_all,
+    k_all,
+    v_all,
+    bias_all,
+    bias_sum,
+    dk_all,
+    dv_all,
     side_send,
     side_recv,
     far_send,
@@ -917,7 +872,9 @@
     partner = me + 1 - 2 * lax.rem(me, 2)
     chunks = held.shape[0]
     block = tokens_ref.shape[1]
-    width = q_ref.shape[1]
+    grain = held.shape[2]
+    length = tokens_ref.shape[0]
+    heads, entries = bias_ref.shape
     pairs = parts // 2
     matrices = (wq_ref, wk_ref, wv_ref)
 
@@ -962,7 +919,7 @@
     pl.semaphore_wait(barrier, parts + 1 + ship)
 
     def rows(chunk):
-        return pl.ds(chunk * REACH, REACH)
+        return pl.ds(chunk * grain, grain)
 
     def far(chunk, away):
         return remote(
@@ -994,6 +951,10 @@
 
     def neighbour():
         return remote(halo, halo_got, halo_send, halo_recv, {"sp": onward})
+
+    scratch = (bias_all, bias_sum, dk_all, dv_all)
+    factor = (q_all.shape[1] // heads) ** (-0.5)
+    work = Attention(factor, heads, q_all, k_all, v_all, g_ref, dq_ref, scratch)
 
     def store(chunk, slot):
         start = pl.multiple_of(order[slot] * block, block)
@@ -1062,7 +1023,8 @@
     for slot in range(2, parts):
         for matrix in range(3):
             load(slot, matrix).wait()
-    outs = (q_ref, k_ref, v_ref)
+    work.begin(exact(bias_ref[...], table_map(entries), 0))
+    waiting = list(range(0, length, ROWS))
     for chunk in backwards:
         for away in range(1, pairs):
             far(chunk, away).wait_recv()
@@ -1079,22 +1041,44 @@
             relay(chunk, away).wait_recv()
             store(chunk, 2 * away + 1).start()
             add(chunk, 2 * away + 1, held[chunk, source(partner, away)])
-        for matrix in range(3):
-            outs[matrix][rows(chunk)] = total[matrix, chunk].astype(jnp.bfloat16)
-        if chunk == chunks - 1:
-            halo[0] = total[1, chunk].astype(jnp.bfloat16)
-            halo[1] = total[2, chunk].astype(jnp.bfloat16)
-            neighbour().start()
-        if ship and chunk + 1 < chunks:
-            ship_copy(chunk + 1, tokens_ref.at[rows(chunk)]).wait_recv()
-            pass_on(chunk + 1).start()
-            keep(chunk + 1, core).start()
-    neighbour().wait()
-    prev_ref[...] = halo_got[...]
+        low = chunk * grain
+        q_all[low : low + grain] = total[0, chunk].astype(jnp.bfloat16)
+        k_all[REACH + low : REACH + low + grain] = total[1, chunk].astype(jnp.bfloat16)
+        v_all[REACH + low : REACH + low + grain] = total[2, chunk].astype(jnp.bfloat16)
+        if low == length - REACH:
+            halo[0] = k_all[length:]
+            halo[1] = v_all[length:]
+
+            @pl.when(seat < seats - 1)
+            def _():
+                neighbour().start()
+
+        while waiting and waiting[-1] >= low + REACH:
+            work.attend(waiting.pop())
+
+    @pl.when(seat > 0)
+    def _():
+        neighbour().wait_recv()
+
+    @pl.when(seat == 0)
+    def _():
+        halo_got[...] = jnp.zeros_like(halo_got)
+
+    k_all[:REACH] = halo_got[0]
+    v_all[:REACH] = halo_got[1]
+    while waiting:
+        work.attend(waiting.pop())
+    work.end(dk_ref, dv_ref, dk_tail_ref, dv_tail_ref, back_ref, line_ref)
+
+    @pl.when(seat < seats - 1)
+    def _():
+        neighbour().wait_send()
+
     if ship:
-        ship_copy(0, tokens_ref.at[rows(0)]).wait_recv()
-        pass_on(0).start()
-        keep(0, core).start()
+        for chunk in backwards:
+            ship_copy(chunk, tokens_ref.at[rows(chunk)]).wait_recv()
+            pass_on(chunk).start()
+            keep(chunk, core).start()
         for chunk in backwards:
             pass_on(chunk).wait_recv()
             keep(chunk, 1 - core).start()
@@ -1112,21 +1096,27 @@
             store(chunk, slot).wait()
 
 
-def project(tokens, query_weight, key_weight, value_weight):
+def attention_grads(tokens, query_weight, key_weight, value_weight, position_bias, out_grad):
     parts = lax.axis_size("tp")
     length, block = tokens.shape
     width = query_weight.shape[1]
-    chunks = length // REACH
+    heads = position_bias.shape[0]
+    chunks = length // GRAIN
     pairs = parts // 2
+    body = length - REACH
     vmem = pl.BlockSpec(memory_space=pltpu.VMEM)
     anywhere = pl.BlockSpec(memory_space=pl.ANY)
-    narrow = jax.ShapeDtypeStruct((length, width), jnp.bfloat16)
+    low = jnp.bfloat16
+
+    def shape(kind, *sizes):
+        return jax.ShapeDtypeStruct(sizes, kind)
+
     dma = pltpu.SemaphoreType.DMA
     ship = paired(lax.axis_size("sp"), parts)
     extra = []
     if ship:
         extra = [
-            pltpu.VMEM((chunks, 2, REACH, block), jnp.bfloat16),
+            pltpu.VMEM((chunks, 2, GRAIN, block), jnp.bfloat16),
             dma((chunks,)),
             dma((chunks,)),
             dma((chunks,)),
@@ -1135,22 +1125,32 @@
         ]
     return pl.pallas_call(
         functools.partial(gather_kernel, parts),
-        in_specs=[vmem, anywhere, anywhere, anywhere],
-        out_specs=[anywhere, vmem, vmem, vmem, vmem, anywhere],
+        in_specs=[vmem, anywhere, anywhere, anywhere, vmem, vmem],
+        out_specs=[anywhere] * 2 + [vmem] * 7,
         out_shape=[
-            jax.ShapeDtypeStruct((length, block * parts), jnp.bfloat16),
-            narrow,
-            narrow,
-            narrow,
-            jax.ShapeDtypeStruct((2, REACH, width), jnp.bfloat16),
-            jax.ShapeDtypeStruct((length, 2 * block) if ship else (8, LANES), jnp.bfloat16),
+            shape(low, length, block * parts),
+            shape(low, *((length, 2 * block) if ship else (8, LANES))),
+            shape(low, length, width),
+            shape(low, body, width),
+            shape(low, body, width),
+            shape(jnp.float32, REACH, width),
+            shape(jnp.float32, REACH, width),
+            shape(low, 2, REACH, width),
+            shape(jnp.float32, heads, TABLE),
         ],
         scratch_shapes=[
-            pltpu.VMEM((chunks, parts, REACH, block), jnp.bfloat16),
+            pltpu.VMEM((chunks, parts, GRAIN, block), low),
             pltpu.VMEM((parts, 3, block, width), jnp.bfloat16),
-            pltpu.VMEM((3, chunks, REACH, width), jnp.float32),
-            pltpu.VMEM((2, REACH, width), jnp.bfloat16),
-            pltpu.VMEM((2, REACH, width), jnp.bfloat16),
+            pltpu.VMEM((3, chunks, GRAIN, width), jnp.float32),
+            pltpu.VMEM((2, REACH, width), low),
+            pltpu.VMEM((2, REACH, width), low),
+            pltpu.VMEM((length, width), low),
+            pltpu.VMEM((length + REACH, width), low),
+            pltpu.VMEM((length + REACH, width), low),
+            pltpu.VMEM((heads, ROWS, WINDOW), jnp.float32),
+            pltpu.VMEM((heads, ROWS, WINDOW), jnp.float32),
+            pltpu.VMEM((length + REACH, width), jnp.float32),
+            pltpu.VMEM((length + REACH, width), jnp.float32),
             dma((chunks,)),
             dma((chunks,)),
             dma((chunks, pairs - 1)),
@@ -1169,27 +1169,24 @@
         cost_estimate=pl.CostEstimate(
             flops=6 * length * block * parts * width, bytes_accessed=150_000_000, transcendentals=0
         ),
-    )(tokens, query_weight, key_weight, value_weight)
+    )(tokens, query_weight, key_weight, value_weight, out_grad, position_bias)
 
 
 def shards(tokens, query_weight, key_weight, value_weight, position_bias, out_grad):
-    whole, query, keys, values, prev, theirs = project(
-        tokens, query_weight, key_weight, value_weight
+    outs = attention_grads(
+        tokens, query_weight, key_weight, value_weight, position_bias, out_grad
     )
-    query_grad, key_body, value_body, key_tail, value_tail, back, lines = attention(
-        query, keys, values, prev, out_grad, position_bias
-    )
-    input_grad, query_weight_grad, key_weight_grad, value_weight_grad, lines = final_grads(
+    whole, theirs, query_grad, key_body, value_body, key_tail, value_tail, back, lines = outs
+    return final_grads(
         whole,
         (theirs,) if paired(lax.axis_size("sp"), lax.axis_size("tp")) else (),
         (query_grad, key_body, value_body),
         (key_tail, value_tail),
         back,
-        lines[:, 0],
+        lines,
         (query_weight, key_weight, value_weight),
+        position_bias.shape[1],
     )
-    bias_grad = table_to_bias(lines, position_bias.shape[1])
-    return input_grad, query_weight_grad, key_weight_grad, value_weight_grad, bias_grad
 
 
 def solution(mesh):

time: 235 us -> 198 us (0.84)
  Pallas kernels: 219 us -> 189 us
  local copies, waits for them, and re-layouts: 12.6 us -> 7.62 us
    pallas_call x1, Pallas kernels: 143 us -> 126 us  [final_grads(): pl.pallas_call(functools.partial(pair_kernel if pair else ring_kernel, co...]
    pallas_call x2 -> x1, Pallas kernels: 75.9 us -> 63.8 us  [attention_grads(): pl.pallas_call(functools.partial(gather_kernel, parts), in_specs=[vmem, a...]
    unnamed x13 -> x11, local copies, waits for them, and re-layouts: 10.1 us -> 7.62 us
where the time goes in v3:
time: 198 us
  Pallas kernels  189 us (95%)
  local copies, waits for them, and re-layouts  7.62 us (4%)
    pallas_call x1, Pallas kernels, final_grads(): pl.pallas_call(functools.partial(pair_kernel if pair else ring_kernel, co...  126 us
    pallas_call x1, Pallas kernels, attention_grads(): pl.pallas_call(functools.partial(gather_kernel, parts), in_specs=[vmem, a...  63.8 us
    unnamed x11, local copies, waits for them, and re-layouts  7.62 us

profile of v3, /device:TPU:0, one launch (start us, length us, event | category | flops | bytes accessed | tf_op | source)
XLA Modules:
  0.0 197.7 jit_solution(85251332551131442)
XLA Ops:
  0.6 63.8 %shard_map.101 = (bf16[768,4096]{1,0:T(8,128)(2,1)}, bf16[768,2048]{1,0:T(8,128)(2,1)}, bf16[768,512]{1,0:T(8,128)(2,1)}, bf16[512,512]{1,0:T(8,128)(2,1)}, bf16...) custom-call(bf16[768,1024]{1,0:T(8,128)(2,1)} %tokens_ref.1, ...), custom_call_target="tpu_custom_call" | custom-call | flops 9663676416 | bytes 150000000 | tf_op jit(solution)/shard_map/pallas_call | solution.py:1126
  64.4 125.6 %shard_map.102 = (bf16[768,1024]{1,0:T(8,128)(2,1)}, f32[512,512]{1,0:T(8,128)}, f32[512,512]{1,0:T(8,128)}, f32[512,512]{1,0:T(8,128)}, f32[4,320]{1,0:T(4,128)}) custom-call(bf16[768,4096]{1,0:T(8,128)(2,1)} %get-tuple-element.14.whole_hbm, bf16[768,512]{1,0:T(8,128)(2,1)} %get-tuple-element.15.dq_hbm, bf16[512,512]{1,0:T(8,128)(2,1)} %get-tuple-element.16.dk_hbm, ...), custom_call_target="tpu_custom_call" | custom-call | flops 19327352832 | bytes 400000000 | tf_op jit(solution)/shard_map/pallas_call | solution.py:805
  190.0 0.0 copy-start.1
  190.0 0.0 copy-start
  190.0 0.0 copy-start.2
  190.1 2.8 %copy.16 = bf16[768,1024]{1,0:T(8,128)(2,1)} copy(bf16[768,1024]{1,0:T(8,128)(2,1)} %get-tuple-element.28) | data formatting | bytes 3145728
  192.9 2.3 %copy.17 = f32[512,512]{1,0:T(8,128)} copy(f32[512,512]{1,0:T(8,128)} %get-tuple-element.29) | data formatting | bytes 2097152
  195.1 0.0 copy-done.1
  195.1 1.0 copy.18
  196.1 0.0 copy-done
  196.1 1.0 copy.19
  197.1 0.0 copy-done.2
  197.1 0.6 copy.20
Async XLA Ops:
  190.0 5.1 %copy-start.1 = (f32[512,512]{1,0:T(8,128)S(1)}, f32[512,512]{1,0:T(8,128)}, u32[]{:S(2)}) copy-start(f32[512,512]{1,0:T(8,128)} %get-tuple-element.30) | copy-start | bytes 3145732
  190.0 6.1 %copy-start = (f32[512,512]{1,0:T(8,128)S(1)}, f32[512,512]{1,0:T(8,128)}, u32[]{:S(2)}) copy-start(f32[512,512]{1,0:T(8,128)} %get-tuple-element.31) | copy-start | bytes 3145732
  190.0 7.0 %copy-start.2 = (f32[4,320]{1,0:T(4,128)S(1)}, f32[4,320]{1,0:T(4,128)}, u32[]{:S(2)}) copy-start(f32[4,320]{1,0:T(4,128)} %get-tuple-element.32) | copy-start | bytes 15364

commit v4 on v3

--- a/solution.py
+++ b/solution.py
@@ -15,7 +15,7 @@
 WINDOW = ROWS + REACH
 TABLE = 512
 LANES = 128
-GRAIN = 256
+GRAIN = 128
 HIDDEN = -1e30
 
 
@@ -110,19 +110,27 @@
             self.dk_all[window, columns] += contract_rows(low, q)
             self.dv_all[window, columns] += contract_rows(weights.astype(jnp.bfloat16), g)
 
-    def end(self, dk_ref, dv_ref, dk_tail_ref, dv_tail_ref, back_ref, line_ref):
+    def behind(self, back):
+        back[0] = (self.dk_all[:REACH] * self.factor).astype(jnp.bfloat16)
+        back[1] = self.dv_all[:REACH].astype(jnp.bfloat16)
+
+    def end(self, dk_ref, dv_ref, line_ref):
         length = self.q_all.shape[0]
+        body = length - REACH
         dk_all, dv_all, factor = self.dk_all, self.dv_all, self.factor
-        back_ref[0] = (dk_all[:REACH] * factor).astype(jnp.bfloat16)
-        back_ref[1] = dv_all[:REACH].astype(jnp.bfloat16)
-        dk_ref[...] = (dk_all[REACH:length] * factor).astype(jnp.bfloat16)
-        dv_ref[...] = dv_all[REACH:length].astype(jnp.bfloat16)
-        dk_tail_ref[...] = dk_all[length:] * factor
-        dv_tail_ref[...] = dv_all[length:]
+        dk_ref[:body] = (dk_all[REACH:length] * factor).astype(jnp.bfloat16)
+        dv_ref[:body] = dv_all[REACH:length].astype(jnp.bfloat16)
         for head in range(self.heads):
             blank = jnp.zeros((ROWS, TABLE - WINDOW), jnp.float32)
             padded = jnp.concatenate([self.bias_sum[head], blank], axis=1)
             line_ref[head : head + 1] = diagonal_sums(padded)
+
+    def join(self, dk_ref, dv_ref, after):
+        length = self.q_all.shape[0]
+        dk = self.dk_all[length:] * self.factor + after[0].astype(jnp.float32)
+        dk_ref[length - REACH :] = dk.astype(jnp.bfloat16)
+        dv = self.dv_all[length:] + after[1].astype(jnp.float32)
+        dv_ref[length - REACH :] = dv.astype(jnp.bfloat16)
 
 
 def ring_columns(count):
@@ -178,62 +186,16 @@
     pl.semaphore_wait(barrier, count + parts - 2)
 
 
-def final_loads(hbm, whole, grads, weights, load_sem):
-    whole_hbm, dq_hbm, dk_hbm, dv_hbm, wq_hbm, wk_hbm, wv_hbm = hbm
-    body = whole.shape[0] - REACH
+def final_loads(hbm, grads, weights, load_sem):
+    dq_hbm, dk_hbm, dv_hbm, wq_hbm, wk_hbm, wv_hbm = hbm
     return [
         pltpu.make_async_copy(dq_hbm, grads.at[0], load_sem.at[0]),
-        pltpu.make_async_copy(dk_hbm, grads.at[1, pl.ds(0, body)], load_sem.at[1]),
-        pltpu.make_async_copy(dv_hbm, grads.at[2, pl.ds(0, body)], load_sem.at[2]),
-        pltpu.make_async_copy(whole_hbm, whole, load_sem.at[3]),
-        pltpu.make_async_copy(wq_hbm, weights.at[0], load_sem.at[4]),
-        pltpu.make_async_copy(wk_hbm, weights.at[1], load_sem.at[5]),
-        pltpu.make_async_copy(wv_hbm, weights.at[2], load_sem.at[6]),
+        pltpu.make_async_copy(dk_hbm, grads.at[1], load_sem.at[1]),
+        pltpu.make_async_copy(dv_hbm, grads.at[2], load_sem.at[2]),
+        pltpu.make_async_copy(wq_hbm, weights.at[0], load_sem.at[3]),
+        pltpu.make_async_copy(wk_hbm, weights.at[1], load_sem.at[4]),
+        pltpu.make_async_copy(wv_hbm, weights.at[2], load_sem.at[5]),
     ]
-
-
-class Halo:
-    def __init__(self, count, grads, tails, back_ref, after, send, recv):
-        self.me = lax.axis_index("sp")
-        self.count = count
-        self.grads, self.tails = grads, tails
-        self.back_ref, self.after, self.sems = back_ref, after, (send, recv)
-
-    def copy(self, which):
-        return remote(
-            self.back_ref.at[which],
-            self.after.at[which],
-            self.sems[0].at[which],
-            self.sems[1].at[which],
-            {"sp": lax.rem(self.me + self.count - 1, self.count)},
-        )
-
-    def start(self):
-        @pl.when(self.me > 0)
-        def _():
-            self.copy(0).start()
-            self.copy(1).start()
-
-    def join(self, which):
-        after = self.after
-
-        @pl.when(self.me < self.count - 1)
-        def _():
-            self.copy(which).wait_recv()
-
-        @pl.when(self.me == self.count - 1)
-        def _():
-            after[which] = jnp.zeros_like(after[which])
-
-        tail = self.tails[which][...] + after[which].astype(jnp.float32)
-        body = self.grads.shape[1] - REACH
-        self.grads[1 + which, body:] = tail.astype(jnp.bfloat16)
-
-    def drain(self):
-        @pl.when(self.me > 0)
-        def _():
-            self.copy(0).wait_send()
-            self.copy(1).wait_send()
 
 
 class Lines:
@@ -363,9 +325,6 @@
     wq_hbm,
     wk_hbm,
     wv_hbm,
-    dk_tail_ref,
-    dv_tail_ref,
-    back_ref,
     line_ref,
     input_ref,
     oq_ref,
@@ -375,7 +334,6 @@
     whole,
     grads,
     weights,
-    after,
     lines,
     pair_sent,
     pair_got,
@@ -383,8 +341,6 @@
     cross_got,
     kept,
     load_sem,
-    back_send,
-    back_recv,
     line_send,
     line_recv,
     pair_send,
@@ -398,14 +354,12 @@
 ):
     me = lax.axis_index("sp")
     place = ring_place(me, count)
-    hbm = (whole_hbm, dq_hbm, dk_hbm, dv_hbm, wq_hbm, wk_hbm, wv_hbm)
-    loads = final_loads(hbm, whole, grads, weights, load_sem)
+    hbm = (dq_hbm, dk_hbm, dv_hbm, wq_hbm, wk_hbm, wv_hbm)
+    loads = final_loads(hbm, grads, weights, load_sem)
+    loads.append(pltpu.make_async_copy(whole_hbm, whole, load_sem.at[6]))
     for load in loads:
         load.start()
     meet(count, parts)
-    halo = Halo(
-        count, grads, (dk_tail_ref, dv_tail_ref), back_ref, after, back_send, back_recv
-    )
     shared = Lines(count, line_ref, line_out_ref, lines, line_send, line_recv)
     buffers = (pair_sent, pair_got, cross_sent, cross_got, kept)
     sems = (pair_send, pair_recv, cross_send, cross_recv)
@@ -436,12 +390,9 @@
             {"sp": onward[side]},
         )
 
-    halo.start()
     for load in loads:
         load.wait()
     for chain in range(3):
-        if chain > 0:
-            halo.join(chain - 1)
         for side in range(2):
             sent[side, chain] = own(target_of(0, side), side, chain).astype(jnp.bfloat16)
             copy_of(sent.at[side, chain], 0, side, chain).start()
@@ -474,8 +425,6 @@
         copy_of(sent.at[side, chain], count - 2, side, chain).wait_recv()
         total = part_of + got[side, chain, count - 2].astype(jnp.float32)
         outs[chain][side * half : (side + 1) * half] = total
-
-    halo.drain()
 
     @pl.loop(0, count - 1)
     def _(step):
@@ -509,19 +458,15 @@
     wk_hbm,
     wv_hbm,
     theirs_hbm,
-    dk_tail_ref,
-    dv_tail_ref,
-    back_ref,
     line_ref,
     input_ref,
     oq_ref,
     ok_ref,
     ov_ref,
     line_out_ref,
-    whole,
+    turned,
     grads,
     weights,
-    after,
     lines,
     pair_sent,
     pair_got,
@@ -529,8 +474,6 @@
     cross_got,
     kept,
     load_sem,
-    back_send,
-    back_recv,
     line_send,
     line_recv,
     pair_send,
@@ -555,15 +498,27 @@
 ):
     me = lax.axis_index("sp")
     level, side, inner, near, made, partner = pair_places(me)
-    hbm = (whole_hbm, dq_hbm, dk_hbm, dv_hbm, wq_hbm, wk_hbm, wv_hbm)
-    loads = final_loads(hbm, whole, grads, weights, load_sem)
-    loads.insert(4, pltpu.make_async_copy(theirs_hbm, theirs, theirs_sem.at[0]))
+    hbm = (dq_hbm, dk_hbm, dv_hbm, wq_hbm, wk_hbm, wv_hbm)
+    loads = final_loads(hbm, grads, weights, load_sem)
+    bands, pairs, _, block = pair_sent.shape
+    length = grads.shape[1]
+
+    def rows(band):
+        return pl.ds(band * REACH, REACH)
+
+    def piece(band, part):
+        start = pl.multiple_of((made * pairs + part) * block, block)
+        return pltpu.make_async_copy(
+            whole_hbm.at[rows(band), pl.ds(start, block)],
+            pair_sent.at[band, part],
+            theirs_sem.at[1 + band * pairs + part],
+        )
+
+    own_loads = [piece(band, part) for band in range(bands) for part in range(pairs)]
+    loads[3:3] = own_loads + [pltpu.make_async_copy(theirs_hbm, theirs, theirs_sem.at[0])]
     for load in loads:
         load.start()
     meet(count, parts)
-    halo = Halo(
-        count, grads, (dk_tail_ref, dv_tail_ref), back_ref, after, back_send, back_recv
-    )
     shared = Lines(count, line_ref, line_out_ref, lines, line_send, line_recv)
     buffers = (pair_sent, pair_got, cross_sent, cross_got, kept)
     sems = (pair_send, pair_recv, cross_send, cross_recv)
@@ -625,12 +580,14 @@
         )
 
     def sums(target, chunk):
-        start = pl.multiple_of(target * depth, depth)
-        mine = whole[:, pl.ds(start, depth)]
         start = pl.multiple_of((target - made * (count // 2)) * depth, depth)
-        their = theirs[:, pl.ds(start, depth)]
-        term = contract_rows(mine, grads[chunk // per, :, columns(chunk)])
-        return term + contract_rows(their, their_grads[chunk // per, :, columns(chunk)])
+        features = pl.ds(start, depth)
+        mine = grads[chunk // per, :, columns(chunk)]
+        other = their_grads[chunk // per, :, columns(chunk)]
+        term = jnp.dot(turned[features, :length], mine, preferred_element_type=jnp.float32)
+        return term + jnp.dot(
+            turned[features, length:], other, preferred_element_type=jnp.float32
+        )
 
     def halve(chunk):
         swap(chunk).wait_recv()
@@ -683,19 +640,23 @@
             def _():
                 store(chunk, matrix).start()
 
-    halo.start()
-    loads[0].wait()
-    for chunk in range(per):
-        swap(chunk).start()
-    for which in range(2):
-        loads[1 + which].wait()
-        halo.join(which)
+    for which in range(3):
+        loads[which].wait()
         for chunk in range(per):
-            swap((1 + which) * per + chunk).start()
+            swap(which * per + chunk).start()
     for load in loads[3:]:
         load.wait()
     shared.start()
 
+    @pl.loop(0, bands)
+    def _(band):
+        start = pl.multiple_of(band * REACH, REACH)
+        for part in range(pairs):
+            low = slice(part * block, (part + 1) * block)
+            turned[low, pl.ds(start, REACH)] = pair_sent[band, part].T
+            turned[low, pl.ds(length + start, REACH)] = theirs[pl.ds(start, REACH), low].T
+
+    hold = 2
     lag = 3 * chunks // 4
 
     @pl.loop(0, chunks + lag)
@@ -704,9 +665,9 @@
         def _():
             halve(step)
 
-        @pl.when((step > 0) & (step <= chunks))
-        def _():
-            onward(step - 1)
+        @pl.when((step >= hold) & (step < chunks + hold))
+        def _():
+            onward(step - hold)
 
         @pl.when(step >= lag)
         def _():
@@ -722,8 +683,6 @@
         grad_in.work(unit)
     shared.finish()
     grad_in.finish(grad_in.bands - 1)
-    halo.drain()
-
     @pl.loop(0, chunks)
     def _(chunk):
         swap(chunk).wait_send()
@@ -738,7 +697,7 @@
     grad_in.drain()
 
 
-def final_grads(whole, theirs, grads, tails, back, lines, weights, entries):
+def final_grads(whole, theirs, grads, lines, weights, entries):
     count = lax.axis_size("sp")
     parts = lax.axis_size("tp")
     pairs = parts // 2
@@ -753,11 +712,12 @@
     dma = pltpu.SemaphoreType.DMA
     low = jnp.bfloat16
     pair = paired(count, parts)
+    tile = min(width, LANES)
+    chunks = 3 * width // tile
     scratch = [
-        pltpu.VMEM((length, features), low),
+        pltpu.VMEM((features // 2, 2 * length) if pair else (length, features), low),
         pltpu.VMEM((3, length, width), low),
         pltpu.VMEM((3, features, width), low),
-        pltpu.VMEM((2, REACH, width), low),
         pltpu.VMEM((count - 1,) + lines.shape, jnp.float32),
         pltpu.VMEM((bands, pairs, REACH, block), low),
         pltpu.VMEM((bands, pairs, REACH, block), low),
@@ -765,8 +725,6 @@
         pltpu.VMEM((bands, pairs - 1, REACH, block), low),
         pltpu.VMEM((bands, REACH, block), jnp.float32),
         dma((7,)),
-        dma((2,)),
-        dma((2,)),
         dma((count - 1,)),
         dma((count - 1,)),
         dma((bands, pairs)),
@@ -775,8 +733,6 @@
         dma((bands, pairs - 1)),
     ]
     if pair:
-        tile = min(width, LANES)
-        chunks = 3 * width // tile
         scratch += [
             pltpu.VMEM((length, features // 2), low),
             pltpu.VMEM((3, length, width), low),
@@ -785,7 +741,7 @@
             pltpu.VMEM((2, chunks, depth, tile), low),
             pltpu.VMEM((2, chunks, depth, tile), low),
             pltpu.VMEM((3, depth, width), jnp.float32),
-            dma((1,)),
+            dma((1 + bands * pairs,)),
             dma((chunks,)),
             dma((chunks,)),
             dma((chunks,)),
@@ -804,7 +760,7 @@
     place = anywhere if pair else vmem
     return pl.pallas_call(
         functools.partial(pair_kernel if pair else ring_kernel, count, parts),
-        in_specs=[anywhere] * (7 + pair) + [vmem] * 4,
+        in_specs=[anywhere] * (7 + pair) + [vmem],
         out_specs=[vmem] + [place] * 3 + [vmem],
         out_shape=[
             jax.ShapeDtypeStruct((length, block), low),
@@ -822,7 +778,7 @@
             bytes_accessed=400_000_000,
             transcendentals=0,
         ),
-    )(whole, *grads, *weights, *theirs, *tails, back, lines)
+    )(whole, *grads, *weights, *theirs, lines)
 
 
 def gather_kernel(
@@ -838,15 +794,14 @@
     dq_ref,
     dk_ref,
     dv_ref,
-    dk_tail_ref,
-    dv_tail_ref,
-    back_ref,
     line_ref,
     held,
     weights,
     total,
     halo,
     halo_got,
+    back,
+    after,
     q_all,
     k_all,
     v_all,
@@ -862,6 +817,8 @@
     relay_recv,
     halo_send,
     halo_recv,
+    back_send,
+    back_recv,
     load_sem,
     store_sem,
     *ship_refs,
@@ -952,6 +909,10 @@
     def neighbour():
         return remote(halo, halo_got, halo_send, halo_recv, {"sp": onward})
 
+    def behind():
+        device = {"sp": lax.rem(seat + seats - 1, seats)}
+        return remote(back, after, back_send, back_recv, device)
+
     scratch = (bias_all, bias_sum, dk_all, dv_all)
     factor = (q_all.shape[1] // heads) ** (-0.5)
     work = Attention(factor, heads, q_all, k_all, v_all, g_ref, dq_ref, scratch)
@@ -1000,21 +961,16 @@
                 keep_sem.at[chunk, which],
             )
 
-    backwards = list(range(chunks))[::-1]
-    for chunk in backwards:
+    tail = REACH // grain
+    sequence = list(range(chunks - tail, chunks)) + list(range(chunks - tail))
+    for chunk in sequence:
         for away in range(1, pairs):
             far(chunk, away).start()
         side(chunk).start()
-        if ship:
-
-            @pl.when(ready)
-            def _():
-                ship_copy(chunk, tokens_ref.at[rows(chunk)]).start()
-
     for slot in range(2):
         for matrix in range(3):
             load(slot, matrix).wait()
-        for chunk in backwards:
+        for chunk in sequence:
             if slot == 1:
                 side(chunk).wait_recv()
             store(chunk, slot).start()
@@ -1024,12 +980,50 @@
         for matrix in range(3):
             load(slot, matrix).wait()
     work.begin(exact(bias_ref[...], table_map(entries), 0))
+    done = []
     waiting = list(range(0, length, ROWS))
-    for chunk in backwards:
+
+    def attend_ready(early):
+        known = {row for chunk in done for row in range(chunk * grain, (chunk + 1) * grain, ROWS)}
+        for start in list(waiting):
+            needs = range(max(0, start - REACH), start + ROWS, ROWS)
+            if start < REACH and early:
+                continue
+            if set(needs) <= known:
+                if start == 0:
+                    take_halo()
+                work.attend(start)
+                waiting.remove(start)
+                if start == REACH - ROWS:
+                    send_behind()
+
+    def take_halo():
+        @pl.when(seat > 0)
+        def _():
+            neighbour().wait_recv()
+
+        @pl.when(seat == 0)
+        def _():
+            halo_got[...] = jnp.zeros_like(halo_got)
+
+        k_all[:REACH] = halo_got[0]
+        v_all[:REACH] = halo_got[1]
+
+    def send_behind():
+        @pl.when(seat > 0)
+        def _():
+            work.behind(back)
+            behind().start()
+
+    for chunk in sequence:
         for away in range(1, pairs):
             far(chunk, away).wait_recv()
             relay(chunk, away).start()
             if ship:
+
+                @pl.when(ready)
+                def _():
+                    ship_copy(chunk, tokens_ref.at[rows(chunk)]).start()
 
                 @pl.when(jnp.logical_not(ready))
                 def _():
@@ -1045,7 +1039,8 @@
         q_all[low : low + grain] = total[0, chunk].astype(jnp.bfloat16)
         k_all[REACH + low : REACH + low + grain] = total[1, chunk].astype(jnp.bfloat16)
         v_all[REACH + low : REACH + low + grain] = total[2, chunk].astype(jnp.bfloat16)
-        if low == length - REACH:
+        done.append(chunk)
+        if chunk == chunks - 1:
             halo[0] = k_all[length:]
             halo[1] = v_all[length:]
 
@@ -1053,41 +1048,42 @@
             def _():
                 neighbour().start()
 
-        while waiting and waiting[-1] >= low + REACH:
-            work.attend(waiting.pop())
+        attend_ready(len(done) < chunks - 1)
+    attend_ready(False)
+    work.end(dk_ref, dv_ref, line_ref)
+
+    @pl.when(seat < seats - 1)
+    def _():
+        behind().wait_recv()
+
+    @pl.when(seat == seats - 1)
+    def _():
+        after[...] = jnp.zeros_like(after)
+
+    work.join(dk_ref, dv_ref, after)
 
     @pl.when(seat > 0)
     def _():
-        neighbour().wait_recv()
-
-    @pl.when(seat == 0)
-    def _():
-        halo_got[...] = jnp.zeros_like(halo_got)
-
-    k_all[:REACH] = halo_got[0]
-    v_all[:REACH] = halo_got[1]
-    while waiting:
-        work.attend(waiting.pop())
-    work.end(dk_ref, dv_ref, dk_tail_ref, dv_tail_ref, back_ref, line_ref)
+        behind().wait_send()
 
     @pl.when(seat < seats - 1)
     def _():
         neighbour().wait_send()
 
     if ship:
-        for chunk in backwards:
+        for chunk in sequence:
             ship_copy(chunk, tokens_ref.at[rows(chunk)]).wait_recv()
             pass_on(chunk).start()
             keep(chunk, core).start()
-        for chunk in backwards:
+        for chunk in sequence:
             pass_on(chunk).wait_recv()
             keep(chunk, 1 - core).start()
-        for chunk in backwards:
+        for chunk in sequence:
             ship_copy(chunk, tokens_ref.at[rows(chunk)]).wait_send()
             pass_on(chunk).wait_send()
             keep(chunk, core).wait()
             keep(chunk, 1 - core).wait()
-    for chunk in backwards:
+    for chunk in sequence:
         side(chunk).wait_send()
         for away in range(1, pairs):
             far(chunk, away).wait_send()
@@ -1103,7 +1099,6 @@
     heads = position_bias.shape[0]
     chunks = length // GRAIN
     pairs = parts // 2
-    body = length - REACH
     vmem = pl.BlockSpec(memory_space=pltpu.VMEM)
     anywhere = pl.BlockSpec(memory_space=pl.ANY)
     low = jnp.bfloat16
@@ -1126,22 +1121,21 @@
     return pl.pallas_call(
         functools.partial(gather_kernel, parts),
         in_specs=[vmem, anywhere, anywhere, anywhere, vmem, vmem],
-        out_specs=[anywhere] * 2 + [vmem] * 7,
+        out_specs=[anywhere] * 2 + [vmem] * 4,
         out_shape=[
             shape(low, length, block * parts),
             shape(low, *((length, 2 * block) if ship else (8, LANES))),
             shape(low, length, width),
-            shape(low, body, width),
-            shape(low, body, width),
-            shape(jnp.float32, REACH, width),
-            shape(jnp.float32, REACH, width),
-            shape(low, 2, REACH, width),
+            shape(low, length, width),
+            shape(low, length, width),
             shape(jnp.float32, heads, TABLE),
         ],
         scratch_shapes=[
             pltpu.VMEM((chunks, parts, GRAIN, block), low),
             pltpu.VMEM((parts, 3, block, width), jnp.bfloat16),
             pltpu.VMEM((3, chunks, GRAIN, width), jnp.float32),
+            pltpu.VMEM((2, REACH, width), low),
+            pltpu.VMEM((2, REACH, width), low),
             pltpu.VMEM((2, REACH, width), low),
             pltpu.VMEM((2, REACH, width), low),
             pltpu.VMEM((length, width), low),
@@ -1159,6 +1153,8 @@
             dma((chunks, pairs - 1)),
             dma(()),
             dma(()),
+            dma(()),
+            dma(()),
             dma((parts, 3)),
             dma((chunks, parts)),
         ]
@@ -1176,17 +1172,38 @@
     outs = attention_grads(
         tokens, query_weight, key_weight, value_weight, position_bias, out_grad
     )
-    whole, theirs, query_grad, key_body, value_body, key_tail, value_tail, back, lines = outs
-    return final_grads(
+    whole, theirs, query_grad, key_grad, value_grad, lines = outs
+    *large, bias_grad = final_grads(
         whole,
         (theirs,) if paired(lax.axis_size("sp"), lax.axis_size("tp")) else (),
-        (query_grad, key_body, value_body),
-        (key_tail, value_tail),
-        back,
+        (query_grad, key_grad, value_grad),
         lines,
         (query_weight, key_weight, value_weight),
         position_bias.shape[1],
     )
+    return (*hand_on(large), bias_grad)
+
+
+def hand_kernel(*refs):
+    half = len(refs) // 2
+    for source, target in zip(refs[:half], refs[half:]):
+        target[...] = source[...]
+
+
+def hand_on(arrays, steps=4):
+    specs = [
+        pl.BlockSpec((array.shape[0] // steps, array.shape[1]), lambda i: (i, 0))
+        for array in arrays
+    ]
+    size = sum(2 * array.size * array.dtype.itemsize for array in arrays)
+    return pl.pallas_call(
+        hand_kernel,
+        grid=(steps,),
+        in_specs=specs,
+        out_specs=specs,
+        out_shape=[jax.ShapeDtypeStruct(array.shape, array.dtype) for array in arrays],
+        cost_estimate=pl.CostEstimate(flops=0, bytes_accessed=size, transcendentals=0),
+    )(*arrays)
 
 
 def solution(mesh):

time: 198 us -> 180 us (0.909)
  Pallas kernels: 189 us -> 178 us
  local copies, waits for them, and re-layouts: 7.62 us -> 0.6 us
    pallas_call x1, Pallas kernels: 126 us -> 107 us  [final_grads(): pl.pallas_call(functools.partial(pair_kernel if pair else ring_kernel, co...]
    unnamed x11 -> x3, local copies, waits for them, and re-layouts: 7.62 us -> 0.6 us
    pallas_call x0 -> x1, Pallas kernels: none -> 4.95 us  [hand_on(): pl.pallas_call(hand_kernel, grid=(steps,), in_specs=specs, out_specs=spec...]
    pallas_call x1, Pallas kernels: 63.8 us -> 66.4 us  [attention_grads(): pl.pallas_call(functools.partial(gather_kernel, parts), in_specs=[vmem, a...]
where the time goes in v4:
time: 180 us
  Pallas kernels  178 us (99%)
    pallas_call x1, Pallas kernels, final_grads(): pl.pallas_call(functools.partial(pair_kernel if pair else ring_kernel, co...  107 us
    pallas_call x1, Pallas kernels, attention_grads(): pl.pallas_call(functools.partial(gather_kernel, parts), in_specs=[vmem, a...  66.4 us
    pallas_call x1, Pallas kernels, hand_on(): pl.pallas_call(hand_kernel, grid=(steps,), in_specs=specs, out_specs=spec...  4.95 us

profile of v4, /device:TPU:0, one launch (start us, length us, event | category | flops | bytes accessed | tf_op | source)
XLA Modules:
  0.0 179.5 jit_solution(11704891112926754799)
XLA Ops:
  0.6 66.4 %shard_map.101 = (bf16[768,4096]{1,0:T(8,128)(2,1)}, bf16[768,2048]{1,0:T(8,128)(2,1)}, bf16[768,512]{1,0:T(8,128)(2,1)}, bf16[768,512]{1,0:T(8,128)(2,1)}, bf16[768,512]{1,0:T(8,128)(2,1)}, /*index=5*/f32[4,512]{1,0:T(4,128)}) custom-call(bf16[768,1024]{1,0:T(8,128)(2,1)} %tokens_ref.1, bf16[4096,512]{1,0:T(8,128)(2,1)} %wq_hbm.1, ...), custom_call_target="tpu_custom_call" | custom-call | flops 9663676416 | bytes 150000000 | tf_op jit(solution)/shard_map/pallas_call | solution.py:1121
  67.0 106.9 %shard_map.102 = (bf16[768,1024]{1,0:T(8,128)(2,1)}, f32[512,512]{1,0:T(8,128)}, f32[512,512]{1,0:T(8,128)}, f32[512,512]{1,0:T(8,128)}, f32[4,320]{1,0:T(4,128)}) custom-call(bf16[768,4096]{1,0:T(8,128)(2,1)} %get-tuple-element.20.whole_hbm, bf16[768,512]{1,0:T(8,128)(2,1)} %get-tuple-element.21.dq_hbm, bf16[768,512]{1,0:T(8,128)(2,1)} %get-tuple-element.22.dk_hbm, ...), custom_call_target="tpu_custom_call" | custom-call | flops 19327352832 | bytes 400000000 | tf_op jit(solution)/shard_map/pallas_call | solution.py:761
  174.0 0.0 copy-start
  174.0 5.0 %shard_map.103 = (bf16[768,1024]{1,0:T(8,128)(2,1)}, f32[512,512]{1,0:T(8,128)}, f32[512,512]{1,0:T(8,128)}, f32[512,512]{1,0:T(8,128)}) custom-call(bf16[768,1024]{1,0:T(8,128)(2,1)} %get-tuple-element.26.refs_0_, f32[512,512]{1,0:T(8,128)} %get-tuple-element.27.refs_1_, f32[512,512]{1,0:T(8,128)} %get-tuple-element.28.refs_2_, ...), custom_call_target="tpu_custom_call" | custom-call | bytes 9437184 | tf_op jit(solution)/shard_map/pallas_call | solution.py:1199
  178.9 0.0 copy-done
  178.9 0.6 copy.12
Async XLA Ops:
  174.0 5.0 %copy-start = (f32[4,320]{1,0:T(4,128)S(1)}, f32[4,320]{1,0:T(4,128)}, u32[]{:S(2)}) copy-start(f32[4,320]{1,0:T(4,128)} %get-tuple-element.44) | copy-start | bytes 15364

commit v5 on v4

--- a/solution.py
+++ b/solution.py
@@ -82,7 +82,7 @@
             self.bias_all[head] = jnp.where(seen, bias, HIDDEN)
 
     def attend(self, start):
-        @pl.loop(0, self.heads)
+        @pl.loop(0, self.heads, unroll=2)
         def _(head):
             columns = pl.ds(pl.multiple_of(head * self.head, self.head), self.head)
             rows = slice(start, start + ROWS)
@@ -606,7 +606,6 @@
         @pl.when(inner)
         def _():
             sent[1, chunk] = term.astype(jnp.bfloat16)
-            rim_copy(chunk).start()
 
         @pl.when(jnp.logical_not(inner))
         def _():
@@ -644,9 +643,9 @@
         loads[which].wait()
         for chunk in range(per):
             swap(which * per + chunk).start()
-    for load in loads[3:]:
+    shared.start()
+    for load in loads[3:-3]:
         load.wait()
-    shared.start()
 
     @pl.loop(0, bands)
     def _(band):
@@ -657,6 +656,7 @@
             turned[low, pl.ds(length + start, REACH)] = theirs[pl.ds(start, REACH), low].T
 
     hold = 2
+    rest = hold + 3
     lag = 3 * chunks // 4
 
     @pl.loop(0, chunks + lag)
@@ -669,11 +669,25 @@
         def _():
             onward(step - hold)
 
+        @pl.when(inner & (step >= rest) & (step < chunks + hold))
+        def _():
+            rim_copy(step - rest).start()
+
+        @pl.when(inner & (step == chunks + hold))
+        def _():
+            for chunk in range(chunks + hold - rest, chunks):
+                rim_copy(chunk).start()
+
         @pl.when(step >= lag)
         def _():
             finish(step - lag)
 
         unit = (step - 1) // 2
+
+        @pl.when(step == 1)
+        def _():
+            for load in loads[-3:]:
+                load.wait()
 
         @pl.when((lax.rem(step, 2) == 1) & (unit < grad_in.units))
         def _():
@@ -683,6 +697,7 @@
         grad_in.work(unit)
     shared.finish()
     grad_in.finish(grad_in.bands - 1)
+
     @pl.loop(0, chunks)
     def _(chunk):
         swap(chunk).wait_send()
@@ -1190,9 +1205,9 @@
         target[...] = source[...]
 
 
-def hand_on(arrays, steps=4):
+def hand_on(arrays, steps=2):
     specs = [
-        pl.BlockSpec((array.shape[0] // steps, array.shape[1]), lambda i: (i, 0))
+        pl.BlockSpec((array.shape[0], array.shape[1] // steps), lambda i: (0, i))
         for array in arrays
     ]
     size = sum(2 * array.size * array.dtype.itemsize for array in arrays)

time: 180 us -> 172 us (0.956)
  Pallas kernels: 178 us -> 170 us
    pallas_call x1, Pallas kernels: 107 us -> 101 us  [final_grads(): pl.pallas_call(functools.partial(pair_kernel if pair else ring_kernel, co...]
where the time goes in v5:
time: 172 us
  Pallas kernels  170 us (99%)
    pallas_call x1, Pallas kernels, final_grads(): pl.pallas_call(functools.partial(pair_kernel if pair else ring_kernel, co...  101 us
    pallas_call x1, Pallas kernels, attention_grads(): pl.pallas_call(functools.partial(gather_kernel, parts), in_specs=[vmem, a...  65.9 us
    pallas_call x1, Pallas kernels, hand_on(): pl.pallas_call(hand_kernel, grid=(steps,), in_specs=specs, out_specs=spec...  3.94 us

profile of v5, /device:TPU:0, one launch (start us, length us, event | category | flops | bytes accessed | tf_op | source)
XLA Modules:
  0.0 171.7 jit_solution(8722169872286748748)
XLA Ops:
  0.6 65.9 %shard_map.101 = (bf16[768,4096]{1,0:T(8,128)(2,1)}, bf16[768,2048]{1,0:T(8,128)(2,1)}, bf16[768,512]{1,0:T(8,128)(2,1)}, bf16[768,512]{1,0:T(8,128)(2,1)}, bf16[768,512]{1,0:T(8,128)(2,1)}, /*index=5*/f32[4,512]{1,0:T(4,128)}) custom-call(bf16[768,1024]{1,0:T(8,128)(2,1)} %tokens_ref.1, bf16[4096,512]{1,0:T(8,128)(2,1)} %wq_hbm.1, ...), custom_call_target="tpu_custom_call" | custom-call | flops 9663676416 | bytes 150000000 | tf_op jit(solution)/shard_map/pallas_call | solution.py:1136
  66.6 100.6 %shard_map.102 = (bf16[768,1024]{1,0:T(8,128)(2,1)}, f32[512,512]{1,0:T(8,128)}, f32[512,512]{1,0:T(8,128)}, f32[512,512]{1,0:T(8,128)}, f32[4,320]{1,0:T(4,128)}) custom-call(bf16[768,4096]{1,0:T(8,128)(2,1)} %get-tuple-element.20.whole_hbm, bf16[768,512]{1,0:T(8,128)(2,1)} %get-tuple-element.21.dq_hbm, bf16[768,512]{1,0:T(8,128)(2,1)} %get-tuple-element.22.dk_hbm, ...), custom_call_target="tpu_custom_call" | custom-call | flops 19327352832 | bytes 400000000 | tf_op jit(solution)/shard_map/pallas_call | solution.py:776
  167.1 0.0 copy-start
  167.1 3.9 %shard_map.103 = (bf16[768,1024]{1,0:T(8,128)(2,1)}, f32[512,512]{1,0:T(8,128)}, f32[512,512]{1,0:T(8,128)}, f32[512,512]{1,0:T(8,128)}) custom-call(bf16[768,1024]{1,0:T(8,128)(2,1)} %get-tuple-element.26.refs_0_, f32[512,512]{1,0:T(8,128)} %get-tuple-element.27.refs_1_, f32[512,512]{1,0:T(8,128)} %get-tuple-element.28.refs_2_, ...), custom_call_target="tpu_custom_call" | custom-call | bytes 9437184 | tf_op jit(solution)/shard_map/pallas_call | solution.py:1214
  171.1 0.0 copy-done
  171.1 0.6 copy.12
Async XLA Ops:
  167.1 4.0 %copy-start = (f32[4,320]{1,0:T(4,128)S(1)}, f32[4,320]{1,0:T(4,128)}, u32[]{:S(2)}) copy-start(f32[4,320]{1,0:T(4,128)} %get-tuple-element.44) | copy-start | bytes 15364

commit v6 on v5

--- a/solution.py
+++ b/solution.py
@@ -656,7 +656,7 @@
             turned[low, pl.ds(length + start, REACH)] = theirs[pl.ds(start, REACH), low].T
 
     hold = 2
-    rest = hold + 3
+    rest = hold + 2
     lag = 3 * chunks // 4
 
     @pl.loop(0, chunks + lag)

time: 172 us -> 170 us (0.988)
  Pallas kernels: 170 us -> 168 us
    pallas_call x1, Pallas kernels: 101 us -> 98.3 us  [final_grads(): pl.pallas_call(functools.partial(pair_kernel if pair else ring_kernel, co...]
where the time goes in v6:
time: 170 us; the launch traced here: 169 us
  Pallas kernels  168 us (99%)
    pallas_call x1, Pallas kernels, final_grads(): pl.pallas_call(functools.partial(pair_kernel if pair else ring_kernel, co...  98.3 us
    pallas_call x1, Pallas kernels, attention_grads(): pl.pallas_call(functools.partial(gather_kernel, parts), in_specs=[vmem, a...  65.9 us
    pallas_call x1, Pallas kernels, hand_on(): pl.pallas_call(hand_kernel, grid=(steps,), in_specs=specs, out_specs=spec...  3.94 us

profile of v6, /device:TPU:0, one launch (start us, length us, event | category | flops | bytes accessed | tf_op | source)
XLA Modules:
  0.0 169.4 jit_solution(14708358091268942009)
XLA Ops:
  0.6 65.9 %shard_map.101 = (bf16[768,4096]{1,0:T(8,128)(2,1)}, bf16[768,2048]{1,0:T(8,128)(2,1)}, bf16[768,512]{1,0:T(8,128)(2,1)}, bf16[768,512]{1,0:T(8,128)(2,1)}, bf16[768,512]{1,0:T(8,128)(2,1)}, /*index=5*/f32[4,512]{1,0:T(4,128)}) custom-call(bf16[768,1024]{1,0:T(8,128)(2,1)} %tokens_ref.1, bf16[4096,512]{1,0:T(8,128)(2,1)} %wq_hbm.1, ...), custom_call_target="tpu_custom_call" | custom-call | flops 9663676416 | bytes 150000000 | tf_op jit(solution)/shard_map/pallas_call | solution.py:1136
  66.6 98.3 %shard_map.102 = (bf16[768,1024]{1,0:T(8,128)(2,1)}, f32[512,512]{1,0:T(8,128)}, f32[512,512]{1,0:T(8,128)}, f32[512,512]{1,0:T(8,128)}, f32[4,320]{1,0:T(4,128)}) custom-call(bf16[768,4096]{1,0:T(8,128)(2,1)} %get-tuple-element.20.whole_hbm, bf16[768,512]{1,0:T(8,128)(2,1)} %get-tuple-element.21.dq_hbm, bf16[768,512]{1,0:T(8,128)(2,1)} %get-tuple-element.22.dk_hbm, ...), custom_call_target="tpu_custom_call" | custom-call | flops 19327352832 | bytes 400000000 | tf_op jit(solution)/shard_map/pallas_call | solution.py:776
  164.9 0.0 copy-start
  164.9 3.9 %shard_map.103 = (bf16[768,1024]{1,0:T(8,128)(2,1)}, f32[512,512]{1,0:T(8,128)}, f32[512,512]{1,0:T(8,128)}, f32[512,512]{1,0:T(8,128)}) custom-call(bf16[768,1024]{1,0:T(8,128)(2,1)} %get-tuple-element.26.refs_0_, f32[512,512]{1,0:T(8,128)} %get-tuple-element.27.refs_1_, f32[512,512]{1,0:T(8,128)} %get-tuple-element.28.refs_2_, ...), custom_call_target="tpu_custom_call" | custom-call | bytes 9437184 | tf_op jit(solution)/shard_map/pallas_call | solution.py:1214
  168.8 0.0 copy-done
  168.8 0.6 copy.12
Async XLA Ops:
  164.9 4.0 %copy-start = (f32[4,320]{1,0:T(4,128)S(1)}, f32[4,320]{1,0:T(4,128)}, u32[]{:S(2)}) copy-start(f32[4,320]{1,0:T(4,128)} %get-tuple-element.44) | copy-start | bytes 15364

commit v7 on v6

--- a/solution.py
+++ b/solution.py
@@ -543,12 +543,12 @@
             {"sp": partner},
         )
 
-    def x_copy(chunk):
+    def x_copy(chunk, which):
         return remote(
-            x_sent.at[chunk],
-            x_got.at[chunk],
-            x_send.at[chunk],
-            x_recv.at[chunk],
+            x_sent.at[chunk, which],
+            x_got.at[chunk, which],
+            x_send.at[chunk, which],
+            x_recv.at[chunk, which],
             {"sp": 2 * level + 1 - side},
         )
 
@@ -592,16 +592,19 @@
     def halve(chunk):
         swap(chunk).wait_recv()
         x_sent[chunk, 0] = sums(deep + 1 - side, chunk).astype(jnp.bfloat16)
+        x_copy(chunk, 0).start()
         x_sent[chunk, 1] = sums(rim + 1 - side, chunk).astype(jnp.bfloat16)
-        x_copy(chunk).start()
+        x_copy(chunk, 1).start()
 
     def onward(chunk):
         term = sums(deep + side, chunk)
-        x_copy(chunk).wait_recv()
+        x_copy(chunk, 0).wait_recv()
         term = term + x_got[chunk, 0].astype(jnp.float32)
         sent[0, chunk] = term.astype(jnp.bfloat16)
         deep_copy(chunk).start()
-        term = sums(rim + side, chunk) + x_got[chunk, 1].astype(jnp.float32)
+        term = sums(rim + side, chunk)
+        x_copy(chunk, 1).wait_recv()
+        term = term + x_got[chunk, 1].astype(jnp.float32)
 
         @pl.when(inner)
         def _():
@@ -701,7 +704,8 @@
     @pl.loop(0, chunks)
     def _(chunk):
         swap(chunk).wait_send()
-        x_copy(chunk).wait_send()
+        x_copy(chunk, 0).wait_send()
+        x_copy(chunk, 1).wait_send()
         deep_copy(chunk).wait_send()
         store(chunk, 0).wait()
 
@@ -759,8 +763,8 @@
             dma((1 + bands * pairs,)),
             dma((chunks,)),
             dma((chunks,)),
-            dma((chunks,)),
-            dma((chunks,)),
+            dma((chunks, 2)),
+            dma((chunks, 2)),
             dma((2, chunks)),
             dma((2, chunks)),
             dma((chunks,)),

time: 170 us -> 171 us (level)
  no operation moved by 1% of the time
where the time goes in v7:
time: 171 us; the launch traced here: 170 us
  Pallas kernels  169 us (99%)
    pallas_call x1, Pallas kernels, final_grads(): pl.pallas_call(functools.partial(pair_kernel if pair else ring_kernel, co...  99.3 us
    pallas_call x1, Pallas kernels, attention_grads(): pl.pallas_call(functools.partial(gather_kernel, parts), in_specs=[vmem, a...  65.9 us
    pallas_call x1, Pallas kernels, hand_on(): pl.pallas_call(hand_kernel, grid=(steps,), in_specs=specs, out_specs=spec...  3.94 us

profile of v7, /device:TPU:0, one launch (start us, length us, event | category | flops | bytes accessed | tf_op | source)
XLA Modules:
  0.0 170.4 jit_solution(8310315145496759251)
XLA Ops:
  0.6 65.9 %shard_map.101 = (bf16[768,4096]{1,0:T(8,128)(2,1)}, bf16[768,2048]{1,0:T(8,128)(2,1)}, bf16[768,512]{1,0:T(8,128)(2,1)}, bf16[768,512]{1,0:T(8,128)(2,1)}, bf16[768,512]{1,0:T(8,128)(2,1)}, /*index=5*/f32[4,512]{1,0:T(4,128)}) custom-call(bf16[768,1024]{1,0:T(8,128)(2,1)} %tokens_ref.1, bf16[4096,512]{1,0:T(8,128)(2,1)} %wq_hbm.1, ...), custom_call_target="tpu_custom_call" | custom-call | flops 9663676416 | bytes 150000000 | tf_op jit(solution)/shard_map/pallas_call | solution.py:1140
  66.6 99.3 %shard_map.102 = (bf16[768,1024]{1,0:T(8,128)(2,1)}, f32[512,512]{1,0:T(8,128)}, f32[512,512]{1,0:T(8,128)}, f32[512,512]{1,0:T(8,128)}, f32[4,320]{1,0:T(4,128)}) custom-call(bf16[768,4096]{1,0:T(8,128)(2,1)} %get-tuple-element.20.whole_hbm, bf16[768,512]{1,0:T(8,128)(2,1)} %get-tuple-element.21.dq_hbm, bf16[768,512]{1,0:T(8,128)(2,1)} %get-tuple-element.22.dk_hbm, ...), custom_call_target="tpu_custom_call" | custom-call | flops 19327352832 | bytes 400000000 | tf_op jit(solution)/shard_map/pallas_call | solution.py:780
  165.9 0.0 copy-start
  165.9 3.9 %shard_map.103 = (bf16[768,1024]{1,0:T(8,128)(2,1)}, f32[512,512]{1,0:T(8,128)}, f32[512,512]{1,0:T(8,128)}, f32[512,512]{1,0:T(8,128)}) custom-call(bf16[768,1024]{1,0:T(8,128)(2,1)} %get-tuple-element.26.refs_0_, f32[512,512]{1,0:T(8,128)} %get-tuple-element.27.refs_1_, f32[512,512]{1,0:T(8,128)} %get-tuple-element.28.refs_2_, ...), custom_call_target="tpu_custom_call" | custom-call | bytes 9437184 | tf_op jit(solution)/shard_map/pallas_call | solution.py:1218
  169.8 0.0 copy-done
  169.8 0.6 copy.12
Async XLA Ops:
  165.9 4.0 %copy-start = (f32[4,320]{1,0:T(4,128)S(1)}, f32[4,320]{1,0:T(4,128)}, u32[]{:S(2)}) copy-start(f32[4,320]{1,0:T(4,128)} %get-tuple-element.44) | copy-start | bytes 15364
